TPU v7x, 512 devices: a whole 4x4x16 slice. The times are simulated.
512 devices in a mesh: sp: 64 (over z, y), tp: 8 (over x, core).
Axes of the slice: x: 4, y: 4, z: 16, core: 2. Of those that a mesh axis runs over, the one named last changes fastest.
Arguments:
- tokens: bfloat16 [16384, 2048], P('sp', 'tp'), may hold values from -6 to 6
- norm_gain: float32 [2048], replicated, may hold values from 0.1 to 1.9
- query_weight: bfloat16 [1024, 2048], P('tp'), may hold values from -0.125 to 0.125
- key_weight: bfloat16 [1024, 2048], P('tp'), may hold values from -0.125 to 0.125
- value_weight: bfloat16 [1024, 2048], P('tp'), may hold values from -0.125 to 0.125
- pool_weight: bfloat16 [1024, 2048], P('tp'), may hold values from -0.125 to 0.125
- query_gain: float32 [64], replicated, may hold values from 0.6 to 6
- key_gain: float32 [64], replicated, may hold values from 0.6 to 6
- cum_gate: float32 [16384, 16], P('sp', 'tp'), as said below
- out_pool_weight: bfloat16 [1024, 2048], P(None, 'tp'), may hold values from -0.1875 to 0.1875
- out_attn_weight: bfloat16 [1024, 2048], P(None, 'tp'), may hold values from -0.1875 to 0.1875
Outputs:
- mixed: bfloat16 [16384, 2048], P('sp', 'tp')
Inputs may be any that keep to these rules, and one draw needn't show every extreme that they name: `cum_gate`: in each head the values never rise along the positions.
All inputs are finite; a program needn't handle non-finite values.
Results may differ from a plain program's by a relative error of at most 0.005.
The roundings to bfloat16 on the way count: a program that leaves them out, or rounds other values in their place, can miss the bound.
Values may be sent and summed in bfloat16 or wider, within the bound.
No kernel may reach another device: no remote copies, remote signals or barrier semaphores. Data moves between devices by JAX's collectives and lax.ppermute only.
A program may use at most 64 MiB of HBM per device.

v0:
```python
import math

import jax
import jax.numpy as jnp
from jax import lax
from jax.sharding import PartitionSpec as P

HEAD_DIM = 64
POOL_WIDTH = 1024
POOL_GROUPS = 4


epsilon = 1e-06
masked_fill = -1e30


def sent_to_all(array, axis):
    size = lax.axis_size(axis)
    return lax.all_to_all(
        jnp.broadcast_to(array[None], (size, *array.shape)), axis, 0, 0, tiled=True
    )


def in_order(tiles, dim):
    tiles = jnp.moveaxis(tiles, 0, dim)
    dims = tiles.shape
    return tiles.reshape(*dims[:dim], dims[dim] * dims[dim + 1], *dims[dim + 2 :])


def gather_directly(array, axis, dim):
    tiles = sent_to_all(array, axis)
    return in_order(tiles, dim)


def from_behind(value, axis, steps):
    count = lax.axis_size(axis)
    leading, last = (max(0, -steps), min(count, count - steps))
    return lax.ppermute(value, axis, [(source, source + steps) for source in range(leading, last)])


def side_by_side(arrays, axis, dim, along):
    both = jnp.concatenate(arrays, axis=along)
    filled, at, finished = (lax.all_gather(both, axis, axis=dim, tiled=True), 0, [])
    for a in arrays:
        finished.append(lax.slice_in_dim(filled, at, at + a.shape[along], axis=along))
        at += a.shape[along]
    return tuple(finished)


def in_one_piece(arrays, axis, dim, along):
    ends, at = ([], 0)
    for a in arrays[:-1]:
        at += a.shape[along]
        ends.append(at)
    both = jnp.concatenate(arrays, axis=along)
    return tuple(jnp.split(gather_directly(both, axis, dim), ends, axis=along))


def rms_scale(values, gain):
    return values * lax.rsqrt(jnp.mean(values * values, axis=-1, keepdims=True) + epsilon) * gain


def block_partials(query_rows, query_pos, query_gate, key_rows, value_rows, key_pos, key_gate):
    logits = jnp.einsum("qhd,gkhd->qhgk", query_rows, key_rows, preferred_element_type=jnp.float32)
    logits = logits + query_gate[:, :, None, None] - jnp.transpose(key_gate, (2, 0, 1))[None]
    allowed = key_pos[None, None, :, :] <= query_pos[:, None, None, None]
    logits = jnp.where(allowed, logits, masked_fill)
    block_max = jnp.max(logits, axis=-1)
    weights = jnp.where(allowed, jnp.exp(logits - block_max[..., None]), 0.0)
    totals = jnp.sum(weights, axis=-1)
    numerator = jnp.einsum(
        "qhgk,gkhd->qhgd",
        weights.astype(jnp.bfloat16),
        value_rows,
        preferred_element_type=jnp.float32,
    )
    return (block_max, totals, numerator)


def merge_state(state, partials):
    run_max, run_den, run_acc = state
    block_max, totals, numerator = partials
    new_max = jnp.maximum(run_max, jnp.max(block_max, axis=-1))
    old_scale = jnp.exp(run_max - new_max)
    block_scale = jnp.exp(block_max - new_max[..., None])
    new_den = run_den * old_scale + jnp.sum(block_scale * totals, axis=-1)
    new_acc = run_acc * old_scale[..., None] + jnp.sum(block_scale[..., None] * numerator, axis=2)
    return (new_max, new_den, new_acc)


def empty_state(rows, heads_here):
    return (
        jnp.full((rows, heads_here), masked_fill, jnp.float32),
        jnp.zeros((rows, heads_here), jnp.float32),
        jnp.zeros((rows, heads_here, HEAD_DIM), jnp.float32),
    )


def per_device(
    tokens,
    norm_gain,
    query_weight,
    key_weight,
    value_weight,
    pool_weight,
    query_gain,
    key_gain,
    cum_gate,
    out_pool_weight,
    out_attn_weight,
):
    full_rows = gather_directly(tokens, "tp", 1)
    normed = rms_scale(full_rows.astype(jnp.float32), norm_gain).astype(jnp.bfloat16)
    length = full_rows.shape[0]
    heads_here = cum_gate.shape[1]
    offset = lax.axis_index("sp") * length

    def project(weight):
        return lax.dot_general(
            normed, weight, (((1,), (1,)), ((), ())), preferred_element_type=jnp.float32
        )

    query_heads = (
        rms_scale(project(query_weight).reshape(length, heads_here, HEAD_DIM), query_gain)
        * HEAD_DIM ** (-0.5)
    ).astype(jnp.bfloat16)
    key_heads = rms_scale(
        project(key_weight).reshape(length, heads_here, HEAD_DIM), key_gain
    ).astype(jnp.bfloat16)
    value_heads = project(value_weight).astype(jnp.bfloat16).reshape(length, heads_here, HEAD_DIM)
    pool_input = project(pool_weight).astype(jnp.bfloat16)
    reach = 2**POOL_GROUPS
    rim_rows = from_behind(pool_input[length - reach :], "sp", 1)
    extended = jnp.concatenate([rim_rows, pool_input], axis=0).astype(jnp.float32)
    prefix = jnp.cumsum(extended, axis=0)
    width_here = pool_input.shape[1]
    channel_ids = lax.axis_index("tp") * width_here + jnp.arange(width_here, dtype=jnp.int32)
    group_ids = channel_ids // (POOL_WIDTH // POOL_GROUPS)
    counts = (offset + jnp.arange(1, length + 1, dtype=jnp.int32)).astype(jnp.float32)[:, None]
    current = prefix[reach:]
    pooled_mean = jnp.zeros((length, width_here), jnp.float32)
    for group_index in range(POOL_GROUPS):
        window = 2 ** (group_index + 1)
        lagged = prefix[reach - window : reach - window + length]
        average = (current - lagged) / jnp.minimum(counts, float(window))
        pooled_mean = jnp.where(group_ids[None, :] == group_index, average, pooled_mean)
    pooled = (pooled_mean - extended[reach:]).astype(jnp.bfloat16)
    gate_all = lax.all_gather(cum_gate, "sp", axis=0, tiled=True)
    query_pos = offset + jnp.arange(length, dtype=jnp.int32)
    key_flat = key_heads.reshape(length, heads_here * HEAD_DIM)
    value_flat = value_heads.reshape(length, heads_here * HEAD_DIM)

    def absorb(carried, inputs):
        key_rows, value_rows, key_gate, key_pos = inputs
        partials = block_partials(
            query_heads, query_pos, cum_gate, key_rows, value_rows, key_pos, key_gate
        )
        return (merge_state(carried, partials), None)

    key_piece, value_piece = side_by_side((key_flat, value_flat), "sp", 0, 1)
    shards = key_piece.shape[0] // length
    grouping = math.gcd(shards, 8)
    turns = shards // grouping
    key_groups = key_piece.reshape(turns, grouping, length, heads_here, HEAD_DIM)
    value_groups = value_piece.reshape(turns, grouping, length, heads_here, HEAD_DIM)
    gate_groups = gate_all.reshape(turns, grouping, length, heads_here)
    pos_groups = jnp.arange(shards * length, dtype=jnp.int32).reshape(turns, grouping, length)
    result, _ = lax.scan(
        absorb, empty_state(length, heads_here), (key_groups, value_groups, gate_groups, pos_groups)
    )
    final_max, final_den, final_acc = result
    attended = (
        (final_acc / final_den[..., None])
        .reshape(length, heads_here * HEAD_DIM)
        .astype(jnp.bfloat16)
    )
    pool_full, attn_full = in_one_piece((pooled, attended), "tp", 1, 0)
    output = jnp.dot(pool_full, out_pool_weight, preferred_element_type=jnp.float32) + jnp.dot(
        attn_full, out_attn_weight, preferred_element_type=jnp.float32
    )
    return output.astype(jnp.bfloat16)


def solution(mesh):
    return jax.shard_map(
        per_device,
        mesh=mesh,
        in_specs=(
            P("sp", "tp"),
            P(),
            P("tp", None),
            P("tp", None),
            P("tp", None),
            P("tp", None),
            P(),
            P(),
            P("sp", "tp"),
            P(None, "tp"),
            P(None, "tp"),
        ),
        out_specs=P("sp", "tp"),
        check_vma=False,
    )
```

profile of v0, /device:TPU:1, one launch (start us, length us, event | category | flops | bytes accessed | tf_op | source)
XLA Modules:
  0.0 286.3 jit_solution(11867176884749024739)
XLA Ops:
  6.5 2.0 broadcast_in_dim.86
  8.6 10.3 %all-to-all-start = ((bf16[8,256,256]{2,1,0:T(8,128)(2,1)}), bf16[8,256,256]{2,1,0:T(8,128)(2,1)S(1)}, u32[]{:S(2)}, u32[]{:S(2)}) async-start(bf16[8,256,256]{2,1,0:T(8,128)(2,1)} %broadcast_in_dim.86), calls=%async_computation | async-start | bytes 2097152 | tf_op jit(solution)/shard_map/all_to_all | solution.py:19
  19.6 14.3 %all-to-all-done = bf16[8,256,256]{2,1,0:T(8,128)(2,1)S(1)} async-done(((bf16[8,256,256]{2,1,0:T(8,128)(2,1)}), bf16[8,256,256]{2,1,0:T(8,128)(2,1)S(1)}, u32[]{:S(2)}, u32[]{:S(2)}) %all-to-all-start) | async-done | bytes 1048608 | tf_op jit(solution)/shard_map/all_to_all | solution.py:19
  37.3 78.8 %all_gather.7 = f32[16384,2]{0,1:T(2,128)S(1)} all-gather(f32[256,2]{0,1:T(2,128)S(1)} %copy-done.7), channel_id=1, replica_groups=mesh['sp'=64,'tp'=8] {'sp'}, dimensions={0}, use_global_device_ids=true | all-gather | bytes 133120 | tf_op jit(solution)/shard_map/all_gather | solution.py:148
  116.2 1.8 convolution_convert_fusion.1
  118.1 1.3 collective-permute-start
  120.6 74.0 %all-gather.2.cloned.1.call-done = bf16[16384,256]{0,1:T(8,128)(2,1)} async-done(((bf16[256,256]{0,1:T(8,128)(2,1)}), bf16[16384,256]{0,1:T(8,128)(2,1)}) %all-gather.2.cloned.1.call-update) | async-done | bytes 8388624 | tf_op jit(solution)/shard_map/all_gather | solution.py:43
  194.7 3.9 %fusion.41 = (bf16[16384,128]{0,1:T(8,128)(2,1)S(1)}, bf16[16384,128]{0,1:T(8,128)(2,1)S(1)}) fusion(bf16[16384,256]{0,1:T(8,128)(2,1)} %all-gather.2.cloned.1.call-done), kind=kLoop, calls=%fused_computation.88 | loop fusion | bytes 16777216 | tf_op jit(solution)/shard_map/slice | solution.py:45
  198.6 3.2 %copy.59 = bf16[16,8,64,256]{3,2,1,0:T(8,128)(2,1)} copy(bf16[16,8,64,256]{3,1,2,0:T(8,128)(2,1)S(1)} %bitcast.108) | data formatting | bytes 8388608
  201.8 3.2 %copy.57 = bf16[16,8,64,256]{3,2,1,0:T(8,128)(2,1)} copy(bf16[16,8,64,256]{3,1,2,0:T(8,128)(2,1)S(1)} %bitcast.107) | data formatting | bytes 8388608
  205.0 43.6 %while.15 = (s32[]{:T(128)}, f32[256,2]{0,1:T(2,128)S(1)}, f32[256,2]{0,1:T(2,128)S(1)}, f32[256,2,64]{0,2,1:T(8,128)S(1)}, s32[8,8,256]{2,1,0:T(8,128)S(1)}, /*...) while((s32[]{:T(128)}, f32[256,2]{0,1:T(2,128)S(1)}, ...), condition=%wide.region_11.12_spmd.clone, body=%wide.region_5.11_spmd.clone.sunk | while | flops 281090816 | bytes 18655392 | solution.py:168
  205.5 1.3 constant_dynamic-slice_fusion.3
  206.7 1.4 fusion.64
  209.2 1.1 fusion.68
  210.9 1.3 constant_dynamic-slice_fusion.3
  212.2 1.4 fusion.64
  216.4 1.3 constant_dynamic-slice_fusion.3
  217.7 1.4 fusion.64
  220.1 1.1 fusion.68
  221.8 1.3 constant_dynamic-slice_fusion.3
  223.1 1.4 fusion.64
  227.3 1.3 constant_dynamic-slice_fusion.3
  228.6 1.4 fusion.64
  232.8 1.3 constant_dynamic-slice_fusion.3
  234.0 1.4 fusion.64
  236.5 1.1 fusion.68
  238.2 1.3 constant_dynamic-slice_fusion.3
  239.5 1.4 fusion.64
  243.7 1.3 constant_dynamic-slice_fusion.3
  245.0 1.4 fusion.64
  247.4 1.1 fusion.68
  249.0 29.0 %all_to_all.10 = bf16[8,512,128]{1,2,0:T(8,128)(2,1)S(1)} all-to-all(bf16[8,512,128]{1,2,0:T(8,128)(2,1)S(1)} %broadcast_in_dim.94), channel_id=1, replica_groups=mesh['sp'=64,'tp'=8] {'tp'}, dimensions={0} | all-to-all | bytes 2097152 | tf_op jit(solution)/shard_map/all_to_all | solution.py:19
  (147 shorter events, 23.9 us)
Async XLA Ops:
  6.5 28.9 %copy-start = (bf16[128,2048]{1,0:T(8,128)(2,1)S(1)}, bf16[128,2048]{1,0:T(8,128)(2,1)}, u32[]{:S(2)}) copy-start(bf16[128,2048]{1,0:T(8,128)(2,1)} %param.16) | copy-start | bytes 1572868
  6.5 28.2 %copy-start.6 = (f32[2048]{0:T(1024)S(1)}, f32[2048]{0:T(1024)}, u32[]{:S(2)}) copy-start(f32[2048]{0:T(1024)} %param.14) | copy-start | bytes 24580
  8.6 25.3 %all-to-all-start = ((bf16[8,256,256]{2,1,0:T(8,128)(2,1)}), bf16[8,256,256]{2,1,0:T(8,128)(2,1)S(1)}, u32[]{:S(2)}, u32[]{:S(2)}) async-start(bf16[8,256,256]{2,1,0:T(8,128)(2,1)} %broadcast_in_dim.86), calls=%async_computation | async-start | bytes 2097152 | tf_op jit(solution)/shard_map/all_to_all | solution.py:19
  18.9 175.8 %all-gather.2.cloned.1.call-start = ((), (), s32[]{:S(2)}) async-start(), calls=%async_computation.2 | async-start | bytes 8519680 | tf_op jit(solution)/shard_map/all_gather | solution.py:43
  19.6 16.6 %copy-start.2 = (bf16[128,2048]{1,0:T(8,128)(2,1)S(1)}, bf16[128,2048]{1,0:T(8,128)(2,1)}, u32[]{:S(2)}) copy-start(bf16[128,2048]{1,0:T(8,128)(2,1)} %param.17) | copy-start | bytes 1572868
  34.4 2.1 copy-start.8
  34.7 2.6 copy-start.7
  35.1 1.0 copy-start.1
  35.4 83.9 %copy-start.4 = (bf16[128,2048]{1,0:T(8,128)(2,1)S(1)}, bf16[128,2048]{1,0:T(8,128)(2,1)}, u32[]{:S(2)}) copy-start(bf16[128,2048]{1,0:T(8,128)(2,1)} %param.15) | copy-start | bytes 1572868
  35.4 84.3 %copy-start.9 = (f32[64]{0:T(128)S(1)}, f32[64]{0:T(128)}, u32[]{:S(2)}) copy-start(f32[64]{0:T(128)} %param.19) | copy-start | bytes 772
  118.1 2.0 collective-permute-start
  248.6 29.5 %copy-start.3 = (bf16[1024,256]{1,0:T(8,128)(2,1)S(1)}, bf16[1024,256]{1,0:T(8,128)(2,1)}, u32[]{:S(2)}) copy-start(bf16[1024,256]{1,0:T(8,128)(2,1)} %param.22) | copy-start | bytes 1572868
  248.6 29.8 %copy-start.5 = (bf16[1024,256]{1,0:T(8,128)(2,1)S(1)}, bf16[1024,256]{1,0:T(8,128)(2,1)}, u32[]{:S(2)}) copy-start(bf16[1024,256]{1,0:T(8,128)(2,1)} %param.23) | copy-start | bytes 1572868
Sparse Core Ops, SparseCore 0:
  37.3 157.2 all-gather.1
where the time goes:
time: 287 us; the launch traced here: 286 us
  blocking collectives  108 us (38%)
  waiting for transfers between devices  88.6 us (31%)
  local copies, waits for them, and re-layouts  24.8 us (9%)
  matrix products  24.2 us (8%)
  other arithmetic  14.8 us (5%)
  between operations  13.8 us (5%)
  starting transfers between devices  11.6 us (4%)
    all_gather x1, blocking collectives, per_device(): gate_all = lax.all_gather(cum_gate, 'sp', axis=0, tiled=True)  78.8 us
    all_gather x1, waiting for transfers between devices, side_by_side(): lax.all_gather(both, axis, axis=dim, tiled=True)  74 us
    all_to_all x1, blocking collectives, sent_to_all(): lax.all_to_all(jnp.broadcast_to(array[None], (size, *array.shape)), axis,...  29 us
    all_to_all x1, waiting for transfers between devices, sent_to_all(): lax.all_to_all(jnp.broadcast_to(array[None], (size, *array.shape)), axis,...  14.3 us
    dot_general x8, matrix products, block_partials(): jnp.einsum('qhd,gkhd->qhgk', query_rows, key_rows, preferred_element_type...  11.5 us
    all_to_all x1, starting transfers between devices, sent_to_all(): lax.all_to_all(jnp.broadcast_to(array[None], (size, *array.shape)), axis,...  10.3 us
    dynamic_slice x8, local copies, waits for them, and re-layouts, per_device(): lax.scan(absorb, empty_state(length, heads_here), (key_groups, value_grou...  10.3 us
    dot_general x8, matrix products, block_partials(): jnp.einsum('qhgk,gkhd->qhgd', weights.astype(jnp.bfloat16), value_rows, p...  8.61 us
  transfers between devices with their start and end apart: 3, of which 3 were waited for; matrix products, arithmetic and copies ran while one was open for 1% of the time, Pallas kernels for 0%

commit v1 on v0

v1 whole, which is shorter than its diff:
```python
import jax
import jax.numpy as jnp
import numpy as np
from jax import lax
from jax.experimental import pallas as pl
from jax.experimental.pallas import tpu as pltpu
from jax.sharding import Mesh, PartitionSpec as P

F32 = jnp.float32
BF16 = jnp.bfloat16
HEAD = 64
EPS = 1e-06
NEG = -1e30
ROWS = 256
SUB = 32
NZ, NY, NX, NC = 16, 4, 4, 2
TP = ("x", "c")
SP = ("z", "y")


def iota(shape, dim):
    return lax.broadcasted_iota(jnp.int32, shape, dim)


def dot_t(a, b):
    return lax.dot_general(a, b, (((1,), (1,)), ((), ())), preferred_element_type=F32)


def dot(a, b):
    return lax.dot_general(a, b, (((1,), (0,)), ((), ())), preferred_element_type=F32)


def three_parts(v):
    a = v.astype(BF16).astype(F32)
    b = (v - a).astype(BF16).astype(F32)
    return a, b, (v - a - b).astype(BF16).astype(F32)


def head_scale(v, gain, times):
    parts = []
    for h in range(2):
        w = v[:, h * HEAD : (h + 1) * HEAD]
        w = w * lax.rsqrt(jnp.mean(w * w, axis=-1, keepdims=True) + EPS) * gain
        parts.append(w * times if times else w)
    return parts


def project_kernel(
    where, own, other, gain, wq, wk, wv, wp, qg, kg, gate, msg, pool, normed
):
    c = where[0]
    total = jnp.zeros((ROWS, 1), F32)
    for x in range(NX):
        for ref in (own, other):
            v = ref[x].astype(F32)
            total = total + jnp.sum(v * v, axis=-1, keepdims=True)
    scale = lax.rsqrt(total / 2048.0 + EPS)
    for x in range(NX):
        for k, ref in enumerate((own, other)):
            at = pl.multiple_of((2 * x + (c if k == 0 else 1 - c)) * 256, 256)
            v = ref[x].astype(F32) * scale * gain[:, pl.ds(at, 256)]
            normed[:, pl.ds(at, 256)] = v.astype(BF16)
    rows = normed[...]
    q = head_scale(dot_t(rows, wq[...]), qg[...], HEAD ** (-0.5))
    k = head_scale(dot_t(rows, wk[...]), kg[...], None)
    v = dot_t(rows, wv[...])
    pool[...] = dot_t(rows, wp[...]).astype(BF16)
    for h in range(2):
        kv = jnp.concatenate([k[h], v[:, h * HEAD : (h + 1) * HEAD]], axis=-1).astype(BF16)
        g = three_parts(gate[h : h + 1, :])
        lines = [g[i][:, 128 * j : 128 * (j + 1)] for i in range(3) for j in range(2)]
        lines = jnp.concatenate(lines + [jnp.zeros((10, 128), F32)], axis=0).astype(BF16)
        for s in range(8):
            msg[s, h, 0:32, :] = kv[32 * s : 32 * s + 32]
            a = q[h][32 * s : 32 * s + 16]
            b = q[h][32 * s + 16 : 32 * s + 32]
            msg[s, h, 32:48, :] = jnp.concatenate([a, b], axis=-1).astype(BF16)
            msg[s, h, 48:64, :] = lines


def attend_kernel(where, kx, ko, qy, gates, out, kv, qs, bias, gap, buf):
    y, c, s = where[0], where[1], where[2]
    lane = iota((16, 128), 1)
    for z in range(NZ):
        for x in range(NX):
            kv[pl.ds(pl.multiple_of(z * 256 + 64 * x + 32 * c, 32), 32), :] = kx[x, z]
            kv[pl.ds(pl.multiple_of(z * 256 + 64 * x + 32 - 32 * c, 32), 32), :] = ko[x, z]
        g = gates[z].astype(F32)
        g = g[0:2] + g[2:4] + g[4:6]
        for j in range(2):
            at = (z % 2) * 256 + j * 128
            bias[z // 2, :, at : at + 128] = jnp.broadcast_to(g[j : j + 1], (8, 128))
        for yy in range(NY):
            p = qy[yy, z].astype(F32)
            base = yy * 64 + (z % 2) * 32
            qs[z // 2, base : base + 16, :] = jnp.where(lane < 64, p, 0.0).astype(BF16)
            qs[z // 2, base + 16 : base + 32, :] = jnp.where(
                lane < 64, pltpu.roll(p, 64, 1), 0.0
            ).astype(BF16)
    r = iota((256, 512), 0)
    l = iota((256, 512), 1)
    q_at = (((r // 32) % 2) * 4 + r // 64) * 256 + 32 * s + r % 32
    k_at = ((l // 256) * 4 + y) * 256 + l % 256
    gap[...] = k_at - q_at

    def step(i, carry):
        low = jnp.full((256, 128), NEG, F32)
        tops = [low, low]
        for t in range(9):
            first = t <= i
            qi = jnp.where(first, i, 7 - i)
            j = jnp.where(first, t, t - i - 1)
            keys = kv[pl.ds(pl.multiple_of(j * 512, 512), 512), :]
            logits = dot_t(qs[qi], keys) - bias[j, 0:1, :]
            logits = jnp.where(gap[...] <= 2048 * (qi - j), logits, NEG)
            buf[t] = logits
            m = jnp.maximum(
                jnp.maximum(logits[:, 0:128], logits[:, 128:256]),
                jnp.maximum(logits[:, 256:384], logits[:, 384:512]),
            )
            if t == 0:
                tops[0] = m
            elif t >= 4:
                tops[1] = jnp.maximum(tops[1], m)
            else:
                tops[0] = jnp.where(first, jnp.maximum(tops[0], m), tops[0])
                tops[1] = jnp.where(first, tops[1], jnp.maximum(tops[1], m))
        tops = [jnp.maximum(jnp.max(m, axis=-1, keepdims=True), -1e29) for m in tops]
        zero = jnp.zeros((256, 128), F32)
        sums, accs = [zero, zero], [zero, zero]
        for t in range(9):
            first = t <= i
            j = jnp.where(first, t, t - i - 1)
            keys = kv[pl.ds(pl.multiple_of(j * 512, 512), 512), :]
            if t == 0:
                m = tops[0]
            elif t >= 4:
                m = tops[1]
            else:
                m = jnp.where(first, tops[0], tops[1])
            w = jnp.exp(buf[t] - m)
            n = (w[:, 0:128] + w[:, 128:256]) + (w[:, 256:384] + w[:, 384:512])
            a = dot(w.astype(BF16), keys)
            if t == 0:
                sums[0], accs[0] = n, a
            elif t >= 4:
                sums[1], accs[1] = sums[1] + n, accs[1] + a
            else:
                sums[0] = jnp.where(first, sums[0] + n, sums[0])
                accs[0] = jnp.where(first, accs[0] + a, accs[0])
                sums[1] = jnp.where(first, sums[1], sums[1] + n)
                accs[1] = jnp.where(first, accs[1], accs[1] + a)
        ln = iota((256, 128), 1)
        for k in range(2):
            n = jnp.sum(sums[k], axis=-1, keepdims=True)
            some = n > 0.0
            safe = jnp.where(some, n, 1.0)
            o = pltpu.roll(accs[k] / safe, 64, 1)
            p0, p1, p2 = three_parts(jnp.where(some, tops[k] + jnp.log(safe), NEG))
            tail = jnp.where(ln == 64, p0, jnp.where(ln == 65, p1, p2))
            o = jnp.where(ln < 64, o, jnp.where(ln < 67, tail, 0.0)).astype(BF16)
            m = i if k == 0 else 7 - i
            for yy in range(NY):
                out[yy, pl.ds(pl.multiple_of(m * 64, 64), 64), :] = o[64 * yy : 64 * yy + 64]
        return carry

    lax.fori_loop(0, 4, step, 0)


def merge_kernel(where, parts, rim, cur, out, pooled):
    x, offset = where[0], where[1]
    vals = [parts[k].astype(F32) for k in range(NY)]
    ln = iota((512, 128), 1)
    stat = (ln >= 64) & (ln < 67)
    lses = [jnp.sum(jnp.where(stat, v, 0.0), axis=-1, keepdims=True) for v in vals]
    top = jnp.maximum(jnp.maximum(lses[0], lses[1]), jnp.maximum(lses[2], lses[3]))
    ws = [jnp.exp(v - top) for v in lses]
    den = (ws[0] + ws[1]) + (ws[2] + ws[3])
    o = (ws[0] * vals[0] + ws[1] * vals[1] + ws[2] * vals[2] + ws[3] * vals[3]) / den
    o = o.reshape(16, 2, 16, 128)
    half = iota((16, 16, 128), 2) < 64
    back = pltpu.roll(o[:, 1].reshape(256, 128), 64, 1).reshape(16, 16, 128)
    out[...] = jnp.where(half, o[:, 0], back).astype(BF16)
    now = cur[...].astype(F32)
    ext = jnp.concatenate([rim[...].astype(F32), now], axis=0)
    counts = (offset + iota((ROWS, 128), 0) + 1).astype(F32)
    mean = jnp.zeros((ROWS, 128), F32)
    run = ext
    for g in range(4):
        w = 2 ** (g + 1)
        n = run.shape[0]
        run = run[w // 2 :] + run[: n - w // 2]
        avg = run[run.shape[0] - ROWS :] / jnp.minimum(counts, float(w))
        mean = jnp.where(x == g, avg, mean)
    pooled[...] = (mean - now).astype(BF16)


def output_kernel(where, own, other, wpo, wao, out, pooled, attended):
    c = where[0]
    half = iota((16, 128), 1) < 64
    for x in range(NX):
        for k, ref in enumerate((own, other)):
            s = 2 * x + (c if k == 0 else 1 - c)
            pooled[:, pl.ds(pl.multiple_of(s * 128, 128), 128)] = ref[x, 256:512, :]
            for j in range(8):
                a = ref[x, 32 * j : 32 * j + 16, :].astype(F32)
                b = ref[x, 32 * j + 16 : 32 * j + 32, :].astype(F32)
                u = jnp.where(half, a, pltpu.roll(b, 64, 1)).astype(BF16)
                v = jnp.where(half, pltpu.roll(a, 64, 1), b).astype(BF16)
                at = pl.multiple_of(s * 32, 32)
                attended[pl.ds(at, 16), 128 * j : 128 * j + 128] = u
                attended[pl.ds(at + 16, 16), 128 * j : 128 * j + 128] = v
    out[...] = (dot(pooled[...], wpo[...]) + dot(attended[...], wao[...])).astype(BF16)


VM = pl.BlockSpec(memory_space=pltpu.VMEM)
SM = pl.BlockSpec(memory_space=pltpu.SMEM)


def call(kernel, name, where, ins, outs, scratch, flops):
    shapes = [jax.ShapeDtypeStruct(s, BF16) for s in outs]
    return pl.pallas_call(
        kernel,
        name=name,
        out_shape=shapes,
        in_specs=[SM] + [VM] * len(ins),
        out_specs=[VM] * len(outs),
        scratch_shapes=scratch,
        cost_estimate=pl.CostEstimate(flops=flops, bytes_accessed=2**20, transcendentals=0),
        compiler_params=pltpu.CompilerParams(vmem_limit_bytes=48 * 2**20),
    )(jnp.stack([jnp.asarray(w, jnp.int32) for w in where]), *ins)


def swap(value):
    return lax.ppermute(value, "c", [(0, 1), (1, 0)])


def per_device(
    tokens, norm_gain, wq, wk, wv, wp, query_gain, key_gain, cum_gate, wpo, wao
):
    z, y, x, c = (lax.axis_index(a) for a in ("z", "y", "x", "c"))
    own = lax.all_gather(tokens, "x", axis=0, tiled=False)
    other = swap(own)
    msg, pool = call(
        project_kernel,
        "project",
        (c,),
        (
            own,
            other,
            norm_gain.reshape(1, 2048),
            wq,
            wk,
            wv,
            wp,
            query_gain.reshape(1, HEAD),
            key_gain.reshape(1, HEAD),
            cum_gate.T,
        ),
        [(8, 2, 64, 128), (ROWS, 128)],
        [pltpu.VMEM((ROWS, 2048), BF16)],
        2 * ROWS * 2048 * 512,
    )
    count = NZ * NY
    rim = lax.ppermute(pool[ROWS - 16 :], SP, [(k, k + 1) for k in range(count - 1)])
    heads = lax.all_to_all(msg.reshape(8, 128, 128), TP, 0, 0, tiled=True)
    mine = lax.all_to_all(heads.reshape(16, 64, 128), "z", 0, 0, tiled=True)
    kx = lax.all_gather(mine[:, 0:32], "x", axis=0, tiled=False)
    ko = swap(kx)
    qy = lax.all_gather(mine[:, 32:48], "y", axis=0, tiled=False)
    (parts,) = call(
        attend_kernel,
        "attend",
        (y, c, 2 * x + c),
        (kx, ko, qy, mine[:, 48:64]),
        [(NY, 512, 128)],
        [
            pltpu.VMEM((4096, 128), BF16),
            pltpu.VMEM((8, 256, 128), BF16),
            pltpu.VMEM((8, 8, 512), F32),
            pltpu.VMEM((256, 512), jnp.int32),
            pltpu.VMEM((9, 256, 512), F32),
        ],
        4 * 72 * 256 * 256 * 128,
    )
    parts = lax.all_to_all(parts, "y", 0, 0, tiled=True)
    merged, pooled = call(
        merge_kernel,
        "merge",
        (x, (z * NY + y) * ROWS),
        (parts, rim, pool),
        [(16, 16, 128), (ROWS, 128)],
        [],
        2**20,
    )
    back = lax.all_to_all(merged, "z", 0, 0, tiled=True)
    both = jnp.concatenate([back.reshape(256, 128), pooled], axis=0)
    own = lax.all_gather(both, "x", axis=0, tiled=False)
    other = swap(own)
    (mixed,) = call(
        output_kernel,
        "output",
        (c,),
        (own, other, wpo, wao),
        [(ROWS, 256)],
        [pltpu.VMEM((ROWS, 1024), BF16), pltpu.VMEM((ROWS, 1024), BF16)],
        2 * ROWS * 2048 * 256,
    )
    return mixed


def solution(mesh):
    grid = Mesh(mesh.devices.reshape(NZ, NY, NX, NC), ("z", "y", "x", "c"))
    return jax.shard_map(
        per_device,
        mesh=grid,
        in_specs=(
            P(SP, TP),
            P(),
            P(TP, None),
            P(TP, None),
            P(TP, None),
            P(TP, None),
            P(),
            P(),
            P(SP, TP),
            P(None, TP),
            P(None, TP),
        ),
        out_specs=P(SP, TP),
        check_vma=False,
    )
```

time: 287 us -> 160 us (0.56)
  waiting for transfers between devices: 88.6 us -> 6.52 us
  starting transfers between devices: 11.6 us -> 38.6 us
  matrix products: 24.2 us -> 0 us
  local copies, waits for them, and re-layouts: 24.8 us -> 3.83 us
  Pallas kernels: 0 us -> 16.5 us
  other arithmetic: 14.8 us -> 0.16 us
  blocking collectives: 108 us -> 93.9 us
  between operations: 13.8 us -> 0.14 us
    all_gather x1 -> x0, waiting for transfers between devices: 74 us -> none  [side_by_side(): lax.all_gather(both, axis, axis=dim, tiled=True)]
    all_gather x1 -> x4, blocking collectives: 78.8 us -> 42 us  [the longest x1 11.4 us: per_device(): own = lax.all_gather(tokens, 'x', axis=0, tiled=False)]
    ppermute x1 -> x4, starting transfers between devices: 1.29 us -> 35.2 us  [the longest x3 31.9 us: swap(): return lax.ppermute(value, 'c', [(0, 1), (1, 0)])]
    dot_general x22 -> x0, matrix products: 24.2 us -> none  [the longest x8 11.5 us: block_partials(): jnp.einsum('qhd,gkhd->qhgk', query_rows, key_rows, preferred_element_type...]
    all_to_all x1 -> x3, blocking collectives: 29 us -> 51.9 us  [the longest x1 24.1 us: per_device(): mine = lax.all_to_all(heads.reshape(16, 64, 128), 'z', 0, 0, tiled=True)]
    pallas_call x0 -> x4, Pallas kernels: none -> 16.5 us  [call(): pl.pallas_call(kernel, name=name, out_shape=shapes, in_specs=[SM] + [VM]...]
    all_to_all x1, waiting for transfers between devices: 14.3 us -> 2.83 us  [per_device(): parts = lax.all_to_all(parts, 'y', 0, 0, tiled=True)]
    dynamic_slice x8 -> x0, local copies, waits for them, and re-layouts: 10.3 us -> none  [per_device(): lax.scan(absorb, empty_state(length, heads_here), (key_groups, value_grou...]
  transfers between devices with their start and end apart: 3 -> 5, of which waited for: 3 -> 4; matrix products, arithmetic and copies ran while one was open for 1% -> 0% of each run, Pallas kernels for 0% -> 0%
where the time goes in v1:
time: 160 us
  blocking collectives  93.9 us (59%)
  starting transfers between devices  38.6 us (24%)
  Pallas kernels  16.5 us (10%)
  waiting for transfers between devices  6.52 us (4%)
  local copies, waits for them, and re-layouts  3.83 us (2%)
    ppermute x3, starting transfers between devices, swap(): return lax.ppermute(value, 'c', [(0, 1), (1, 0)])  31.9 us
    all_to_all x1, blocking collectives, per_device(): mine = lax.all_to_all(heads.reshape(16, 64, 128), 'z', 0, 0, tiled=True)  24.1 us
    all_to_all x1, blocking collectives, per_device(): back = lax.all_to_all(merged, 'z', 0, 0, tiled=True)  18.4 us
    pallas_call x4, Pallas kernels, call(): pl.pallas_call(kernel, name=name, out_shape=shapes, in_specs=[SM] + [VM]...  16.5 us
    all_gather x1, blocking collectives, per_device(): own = lax.all_gather(tokens, 'x', axis=0, tiled=False)  11.4 us
    all_gather x1, blocking collectives, per_device(): qy = lax.all_gather(mine[:, 32:48], 'y', axis=0, tiled=False)  10.2 us
    all_gather x1, blocking collectives, per_device(): kx = lax.all_gather(mine[:, 0:32], 'x', axis=0, tiled=False)  10.2 us
    all_gather x1, blocking collectives, per_device(): own = lax.all_gather(both, 'x', axis=0, tiled=False)  10.2 us
  transfers between devices with their start and end apart: 5, of which 4 were waited for; matrix products, arithmetic and copies ran while one was open for 0% of the time, Pallas kernels for 0%

profile of v1, /device:TPU:1, one launch (start us, length us, event | category | flops | bytes accessed | tf_op | source)
XLA Modules:
  0.0 159.6 jit_solution(16350120447651009685)
XLA Ops:
  0.0 11.4 %all-gather = bf16[1024,256]{1,0:T(8,128)(2,1)S(1)} all-gather(bf16[256,256]{1,0:T(8,128)(2,1)} %param.11), channel_id=2, replica_groups=mesh['z'=16,'y'=4,'x'=4,'c'=2] {'x'}, dimensions={0}, use_global_device_ids=true | all-gather | bytes 655360 | tf_op jit(solution)/shard_map/all_gather | solution.py:242
  11.4 10.6 %collective-permute-start = (bf16[4,256,256]{2,1,0:T(8,128)(2,1)S(1)}, bf16[4,256,256]{2,1,0:T(8,128)(2,1)S(1)}, u32[]{:S(2)}, u32[]{:S(2)}) collective-permute-start(bf16[4,256,256]{2,1,0:T(8,128)(2,1)S(1)} %bitcast.18), channel_id=1, source_target_pairs={{0,1},{1,0},{2,3},{3,2},{4,5},{5,4},{6,7},{7,6},{8,9},{9,8},{10,11... | collective-permute-start | bytes 1572872 | tf_op jit(solution)/shard_map/ppermute | solution.py:235
  22.0 1.5 collective-permute-done.other
  23.5 0.0 copy-done.2
  23.5 0.0 copy-done.6
  23.5 0.7 copy-done.7
  24.2 0.0 copy-done.8
  24.2 1.0 copy-done.3
  25.2 1.0 copy-done.4
  26.3 1.0 copy-done.5
  27.3 2.2 %project.1 = (bf16[8,2,64,128]{3,2,1,0:T(8,128)(2,1)S(1)}, bf16[256,128]{1,0:T(8,128)(2,1)S(1)}) custom-call(s32[1]{0:T(128)} %bitcast.where, bf16[4,256,256]{2,1,0:T(8,128)(2,1)S(1)} %bitcast.19, bf16[4,256,256]{2,1,0:T(8,128)(2,1)S(1)} %collective-permute-done.other, f32[1,2048]{1,0:T(1,128)S(1)} %bitcast.24, bf16[128,2048]{1,0:T(8,128)(2,1)S(1)} %copy-done.2, ...), custom_call_target="tpu_custom_call" | custom-call | flops 536870912 | bytes 1048576 | tf_op jit(solution)/shard_map/project/pallas_call | solution.py:222
  29.5 9.4 %all_to_all.20 = bf16[8,128,128]{2,1,0:T(8,128)(2,1)S(1)} all-to-all(bf16[8,128,128]{2,1,0:T(8,128)(2,1)S(1)} %bitcast.23), channel_id=1, replica_groups=mesh['z'=16,'y'=4,'x'=4,'c'=2] {'x','c'}, dimensions={0} | all-to-all | bytes 524288 | tf_op jit(solution)/shard_map/all_to_all | solution.py:266
  38.9 24.1 %all_to_all.21 = bf16[16,64,128]{2,1,0:T(8,128)(2,1)S(1)} all-to-all(bf16[16,64,128]{2,1,0:T(8,128)(2,1)S(1)} %bitcast.28), channel_id=1, replica_groups=mesh['z'=16,'y'=4,'x'=4,'c'=2] {'z'}, dimensions={0} | all-to-all | bytes 524288 | tf_op jit(solution)/shard_map/all_to_all | solution.py:267
  63.1 10.2 %all-gather.1 = bf16[64,32,128]{2,1,0:T(8,128)(2,1)S(1)} all-gather(bf16[16,32,128]{2,1,0:T(8,128)(2,1)S(1)} %slice.16), channel_id=3, replica_groups=mesh['z'=16,'y'=4,'x'=4,'c'=2] {'x'}, dimensions={0}, use_global_device_ids=true | all-gather | bytes 655360 | tf_op jit(solution)/shard_map/all_gather | solution.py:268
  73.3 11.1 %collective-permute-start.1 = (bf16[4,16,32,128]{3,2,1,0:T(8,128)(2,1)S(1)}, bf16[4,16,32,128]{3,2,1,0:T(8,128)(2,1)S(1)}, u32[]{:S(2)}, u32[]{:S(2)}) collective-permute-start(bf16[4,16,32,128]{3,2,1,0:T(8,128)(2,1)S(1)} %bitcast.20), channel_id=1, source_target_pairs={{0,1},{1,0},{2,3},{3,2},{4,5},{5,4},{6,7},{7,6},{8,9},{9,8},{10,11... | collective-permute-start | bytes 1572872 | tf_op jit(solution)/shard_map/ppermute | solution.py:235
  84.4 0.1 pad_add_fusion.1.where
  84.5 10.2 %all-gather.2 = bf16[64,16,128]{2,1,0:T(8,128)(2,1)S(1)} all-gather(bf16[16,16,128]{2,1,0:T(8,128)(2,1)S(1)} %get-tuple-element.14), channel_id=4, replica_groups=mesh['z'=16,'y'=4,'x'=4,'c'=2] {'y'}, dimensions={0}, use_global_device_ids=true | all-gather | bytes 327680 | tf_op jit(solution)/shard_map/all_gather | solution.py:270
  94.7 0.0 collective-permute-done.1.ko
  94.7 11.6 %attend.1 = bf16[4,512,128]{2,1,0:T(8,128)(2,1)} custom-call(s32[3]{0:T(128)S(1)} %pad_add_fusion.1.where, bf16[4,16,32,128]{3,2,1,0:T(8,128)(2,1)S(1)} %bitcast.21, bf16[4,16,32,128]{3,2,1,0:T(8,128)(2,1)S(1)} %collective-permute-done.1.ko, bf16[4,16,16,128]{3,2,1,0:T(8,128)(2,1)S(1)} %bitcast.22, bf16[16,16,128]{2,1,0:T(8,128)(2,1)S(1)} %get-tuple-element.13.gates), custom_call_target="tpu_custom_call" | custom-call | flops 2415919104 | bytes 1048576 | tf_op jit(solution)/shard_map/attend/pallas_call | solution.py:222
  106.3 3.5 %all-to-all-start.2 = ((bf16[4,512,128]{2,1,0:T(8,128)(2,1)}), bf16[4,512,128]{2,1,0:T(8,128)(2,1)S(1)}, u32[]{:S(2)}, u32[]{:S(2)}) async-start(bf16[4,512,128]{2,1,0:T(8,128)(2,1)} %attend.1), calls=%async_computation.2 | async-start | bytes 1048576 | tf_op jit(solution)/shard_map/all_to_all | solution.py:286
  109.8 3.3 %collective-permute-start.2 = (bf16[16,128]{1,0:T(8,128)(2,1)S(1)}, bf16[16,128]{1,0:T(8,128)(2,1)S(1)}, u32[]{:S(2)}, u32[]{:S(2)}) collective-permute-start(bf16[16,128]{1,0:T(8,128)(2,1)S(1)} %slice.15), channel_id=1, source_target_pairs={{0,8},{8,16},{16,24},{24,32},{32,40},{40,48},{48,56},{56,64},{64,7... | collective-permute-start | bytes 12296 | tf_op jit(solution)/shard_map/ppermute | solution.py:265
  113.1 0.1 pad_add_fusion.where
  113.1 0.7 collective-permute-done.2.rim
  113.8 2.8 %all-to-all-done.2.parts = bf16[4,512,128]{2,1,0:T(8,128)(2,1)S(1)} async-done(((bf16[4,512,128]{2,1,0:T(8,128)(2,1)}), bf16[4,512,128]{2,1,0:T(8,128)(2,1)S(1)}, u32[]{:S(2)}, u32[]{:S(2)}) %all-to-all-start.2) | async-done | bytes 524320 | tf_op jit(solution)/shard_map/all_to_all | solution.py:286
  116.6 1.2 merge.1
  117.9 0.0 copy-start
  117.9 0.0 copy-start.1
  117.9 18.4 %all_to_all.22 = bf16[16,16,128]{2,1,0:T(8,128)(2,1)S(1)} all-to-all(bf16[16,16,128]{2,1,0:T(8,128)(2,1)S(1)} %get-tuple-element.11), channel_id=1, replica_groups=mesh['z'=16,'y'=4,'x'=4,'c'=2] {'z'}, dimensions={0} | all-to-all | bytes 131072 | tf_op jit(solution)/shard_map/all_to_all | solution.py:296
  136.3 10.2 %all-gather.3 = bf16[2048,128]{1,0:T(8,128)(2,1)S(1)} all-gather(bf16[512,128]{1,0:T(8,128)(2,1)S(1)} %pad_maximum_fusion), channel_id=5, replica_groups=mesh['z'=16,'y'=4,'x'=4,'c'=2] {'x'}, dimensions={0}, use_global_device_ids=true | all-gather | bytes 655360 | tf_op jit(solution)/shard_map/all_gather | solution.py:298
  146.5 10.2 %collective-permute-start.3 = (bf16[4,512,128]{2,1,0:T(8,128)(2,1)S(1)}, bf16[4,512,128]{2,1,0:T(8,128)(2,1)S(1)}, u32[]{:S(2)}, u32[]{:S(2)}) collective-permute-start(bf16[4,512,128]{2,1,0:T(8,128)(2,1)S(1)} %bitcast.16), channel_id=1, source_target_pairs={{0,1},{1,0},{2,3},{3,2},{4,5},{5,4},{6,7},{7,6},{8,9},{9,8},{10,11... | collective-permute-start | bytes 1572872 | tf_op jit(solution)/shard_map/ppermute | solution.py:235
  156.7 1.5 collective-permute-done.3.other
  158.2 1.4 output.1
  (15 shorter events, 0.1 us)
Async XLA Ops:
  0.0 23.5 %copy-start.2 = (bf16[128,2048]{1,0:T(8,128)(2,1)S(1)}, bf16[128,2048]{1,0:T(8,128)(2,1)}, u32[]{:S(2)}) copy-start(bf16[128,2048]{1,0:T(8,128)(2,1)} %wq.1) | copy-start | bytes 1572868
  11.4 12.1 %copy-start.6 = (f32[2048]{0:T(1024)S(1)}, f32[2048]{0:T(1024)}, u32[]{:S(2)}) copy-start(f32[2048]{0:T(1024)} %param.12) | copy-start | bytes 24580
  11.4 12.1 %collective-permute-start = (bf16[4,256,256]{2,1,0:T(8,128)(2,1)S(1)}, bf16[4,256,256]{2,1,0:T(8,128)(2,1)S(1)}, u32[]{:S(2)}, u32[]{:S(2)}) collective-permute-start(bf16[4,256,256]{2,1,0:T(8,128)(2,1)S(1)} %bitcast.18), channel_id=1, source_target_pairs={{0,1},{1,0},{2,3},{3,2},{4,5},{5,4},{6,7},{7,6},{8,9},{9,8},{10,11... | collective-permute-start | bytes 1572872 | tf_op jit(solution)/shard_map/ppermute | solution.py:235
  23.5 0.7 copy-start.7
  23.5 0.7 copy-start.8
  23.5 0.7 copy-start.9
  24.2 1.0 copy-start.3
  25.2 1.0 copy-start.4
  26.3 1.0 copy-start.5
  73.3 21.4 %collective-permute-start.1 = (bf16[4,16,32,128]{3,2,1,0:T(8,128)(2,1)S(1)}, bf16[4,16,32,128]{3,2,1,0:T(8,128)(2,1)S(1)}, u32[]{:S(2)}, u32[]{:S(2)}) collective-permute-start(bf16[4,16,32,128]{3,2,1,0:T(8,128)(2,1)S(1)} %bitcast.20), channel_id=1, source_target_pairs={{0,1},{1,0},{2,3},{3,2},{4,5},{5,4},{6,7},{7,6},{8,9},{9,8},{10,11... | collective-permute-start | bytes 1572872 | tf_op jit(solution)/shard_map/ppermute | solution.py:235
  106.3 10.4 %all-to-all-start.2 = ((bf16[4,512,128]{2,1,0:T(8,128)(2,1)}), bf16[4,512,128]{2,1,0:T(8,128)(2,1)S(1)}, u32[]{:S(2)}, u32[]{:S(2)}) async-start(bf16[4,512,128]{2,1,0:T(8,128)(2,1)} %attend.1), calls=%async_computation.2 | async-start | bytes 1048576 | tf_op jit(solution)/shard_map/all_to_all | solution.py:286
  109.8 4.0 %collective-permute-start.2 = (bf16[16,128]{1,0:T(8,128)(2,1)S(1)}, bf16[16,128]{1,0:T(8,128)(2,1)S(1)}, u32[]{:S(2)}, u32[]{:S(2)}) collective-permute-start(bf16[16,128]{1,0:T(8,128)(2,1)S(1)} %slice.15), channel_id=1, source_target_pairs={{0,8},{8,16},{16,24},{24,32},{32,40},{40,48},{48,56},{56,64},{64,7... | collective-permute-start | bytes 12296 | tf_op jit(solution)/shard_map/ppermute | solution.py:265
  117.9 40.3 %copy-start = (bf16[1024,256]{1,0:T(8,128)(2,1)S(1)}, bf16[1024,256]{1,0:T(8,128)(2,1)}, u32[]{:S(2)}) copy-start(bf16[1024,256]{1,0:T(8,128)(2,1)} %wpo.1) | copy-start | bytes 1572868
  117.9 40.3 %copy-start.1 = (bf16[1024,256]{1,0:T(8,128)(2,1)S(1)}, bf16[1024,256]{1,0:T(8,128)(2,1)}, u32[]{:S(2)}) copy-start(bf16[1024,256]{1,0:T(8,128)(2,1)} %wao.1) | copy-start | bytes 1572868
  146.5 11.7 %collective-permute-start.3 = (bf16[4,512,128]{2,1,0:T(8,128)(2,1)S(1)}, bf16[4,512,128]{2,1,0:T(8,128)(2,1)S(1)}, u32[]{:S(2)}, u32[]{:S(2)}) collective-permute-start(bf16[4,512,128]{2,1,0:T(8,128)(2,1)S(1)} %bitcast.16), channel_id=1, source_target_pairs={{0,1},{1,0},{2,3},{3,2},{4,5},{5,4},{6,7},{7,6},{8,9},{9,8},{10,11... | collective-permute-start | bytes 1572872 | tf_op jit(solution)/shard_map/ppermute | solution.py:235

commit v2 on v1

--- a/solution.py
+++ b/solution.py
@@ -1,10 +1,10 @@
 import jax
 import jax.numpy as jnp
-import numpy as np
 from jax import lax
 from jax.experimental import pallas as pl
 from jax.experimental.pallas import tpu as pltpu
 from jax.sharding import Mesh, PartitionSpec as P
+
 
 F32 = jnp.float32
 BF16 = jnp.bfloat16
@@ -12,7 +12,6 @@
 EPS = 1e-06
 NEG = -1e30
 ROWS = 256
-SUB = 32
 NZ, NY, NX, NC = 16, 4, 4, 2
 TP = ("x", "c")
 SP = ("z", "y")
@@ -46,9 +45,13 @@
 
 
 def project_kernel(
-    where, own, other, gain, wq, wk, wv, wp, qg, kg, gate, msg, pool, normed
+    where, own, other, gain, wq, wk_, wv_, wp_, qg, kg, gate, msg, pool, normed, wk, wv, wp, sems
 ):
     c = where[0]
+    pairs = ((wk_, wk), (wv_, wv), (wp_, wp))
+    copies = [pltpu.make_async_copy(a, b, sems.at[k]) for k, (a, b) in enumerate(pairs)]
+    for copy in copies:
+        copy.start()
     total = jnp.zeros((ROWS, 1), F32)
     for x in range(NX):
         for ref in (own, other):
@@ -62,6 +65,8 @@
             normed[:, pl.ds(at, 256)] = v.astype(BF16)
     rows = normed[...]
     q = head_scale(dot_t(rows, wq[...]), qg[...], HEAD ** (-0.5))
+    for copy in copies:
+        copy.wait()
     k = head_scale(dot_t(rows, wk[...]), kg[...], None)
     v = dot_t(rows, wv[...])
     pool[...] = dot_t(rows, wp[...]).astype(BF16)
@@ -69,22 +74,21 @@
         kv = jnp.concatenate([k[h], v[:, h * HEAD : (h + 1) * HEAD]], axis=-1).astype(BF16)
         g = three_parts(gate[h : h + 1, :])
         lines = [g[i][:, 128 * j : 128 * (j + 1)] for i in range(3) for j in range(2)]
-        lines = jnp.concatenate(lines + [jnp.zeros((10, 128), F32)], axis=0).astype(BF16)
+        lines = jnp.concatenate(lines + [jnp.zeros((2, 128), F32)], axis=0).astype(BF16)
         for s in range(8):
             msg[s, h, 0:32, :] = kv[32 * s : 32 * s + 32]
             a = q[h][32 * s : 32 * s + 16]
             b = q[h][32 * s + 16 : 32 * s + 32]
             msg[s, h, 32:48, :] = jnp.concatenate([a, b], axis=-1).astype(BF16)
-            msg[s, h, 48:64, :] = lines
-
-
-def attend_kernel(where, kx, ko, qy, gates, out, kv, qs, bias, gap, buf):
-    y, c, s = where[0], where[1], where[2]
+            msg[s, h, 48:56, :] = lines
+
+
+def attend_kernel(where, ks, qy, gates, out, kv, qs, bias, gap, buf):
+    y, s = where[0], where[1]
     lane = iota((16, 128), 1)
     for z in range(NZ):
-        for x in range(NX):
-            kv[pl.ds(pl.multiple_of(z * 256 + 64 * x + 32 * c, 32), 32), :] = kx[x, z]
-            kv[pl.ds(pl.multiple_of(z * 256 + 64 * x + 32 - 32 * c, 32), 32), :] = ko[x, z]
+        for k in range(8):
+            kv[z * 256 + 32 * k : z * 256 + 32 * k + 32, :] = ks[k, z]
         g = gates[z].astype(F32)
         g = g[0:2] + g[2:4] + g[4:6]
         for j in range(2):
@@ -167,8 +171,7 @@
     lax.fori_loop(0, 4, step, 0)
 
 
-def merge_kernel(where, parts, rim, cur, out, pooled):
-    x, offset = where[0], where[1]
+def merge_kernel(where, parts, out):
     vals = [parts[k].astype(F32) for k in range(NY)]
     ln = iota((512, 128), 1)
     stat = (ln >= 64) & (ln < 67)
@@ -181,6 +184,10 @@
     half = iota((16, 16, 128), 2) < 64
     back = pltpu.roll(o[:, 1].reshape(256, 128), 64, 1).reshape(16, 16, 128)
     out[...] = jnp.where(half, o[:, 0], back).astype(BF16)
+
+
+def pool_kernel(where, rim, cur, pooled):
+    x, offset = where[0], where[1]
     now = cur[...].astype(F32)
     ext = jnp.concatenate([rim[...].astype(F32), now], axis=0)
     counts = (offset + iota((ROWS, 128), 0) + 1).astype(F32)
@@ -195,13 +202,13 @@
     pooled[...] = (mean - now).astype(BF16)
 
 
-def output_kernel(where, own, other, wpo, wao, out, pooled, attended):
+def output_kernel(where, own, other, pools, wpo, wao, out, pooled, attended):
     c = where[0]
     half = iota((16, 128), 1) < 64
     for x in range(NX):
         for k, ref in enumerate((own, other)):
             s = 2 * x + (c if k == 0 else 1 - c)
-            pooled[:, pl.ds(pl.multiple_of(s * 128, 128), 128)] = ref[x, 256:512, :]
+            pooled[:, 128 * (2 * x + k) : 128 * (2 * x + k + 1)] = pools[2 * x + k]
             for j in range(8):
                 a = ref[x, 32 * j : 32 * j + 16, :].astype(F32)
                 b = ref[x, 32 * j + 16 : 32 * j + 32, :].astype(F32)
@@ -217,25 +224,33 @@
 SM = pl.BlockSpec(memory_space=pltpu.SMEM)
 
 
-def call(kernel, name, where, ins, outs, scratch, flops):
+HB = pl.BlockSpec(memory_space=pltpu.HBM)
+
+
+def call(kernel, where, ins, outs, scratch, flops, mib, in_hbm=()):
     shapes = [jax.ShapeDtypeStruct(s, BF16) for s in outs]
     return pl.pallas_call(
         kernel,
-        name=name,
         out_shape=shapes,
-        in_specs=[SM] + [VM] * len(ins),
+        in_specs=[SM] + [HB if k in in_hbm else VM for k in range(len(ins))],
         out_specs=[VM] * len(outs),
         scratch_shapes=scratch,
         cost_estimate=pl.CostEstimate(flops=flops, bytes_accessed=2**20, transcendentals=0),
-        compiler_params=pltpu.CompilerParams(vmem_limit_bytes=48 * 2**20),
+        compiler_params=pltpu.CompilerParams(vmem_limit_bytes=mib * 2**20),
     )(jnp.stack([jnp.asarray(w, jnp.int32) for w in where]), *ins)
+
+
+def spread(value, axis):
+    size = lax.axis_size(axis)
+    copies = jnp.broadcast_to(value[None], (size, *value.shape))
+    return lax.all_to_all(copies, axis, 0, 0, tiled=True)
 
 
 def swap(value):
     return lax.ppermute(value, "c", [(0, 1), (1, 0)])
 
 
-def per_device(
+def layer(
     tokens, norm_gain, wq, wk, wv, wp, query_gain, key_gain, cum_gate, wpo, wao
 ):
     z, y, x, c = (lax.axis_index(a) for a in ("z", "y", "x", "c"))
@@ -243,7 +258,6 @@
     other = swap(own)
     msg, pool = call(
         project_kernel,
-        "project",
         (c,),
         (
             own,
@@ -257,22 +271,28 @@
             key_gain.reshape(1, HEAD),
             cum_gate.T,
         ),
-        [(8, 2, 64, 128), (ROWS, 128)],
-        [pltpu.VMEM((ROWS, 2048), BF16)],
+        [(8, 2, 56, 128), (ROWS, 128)],
+        [pltpu.VMEM((ROWS, 2048), BF16)]
+        + [pltpu.VMEM((128, 2048), BF16)] * 3
+        + [pltpu.SemaphoreType.DMA((3,))],
         2 * ROWS * 2048 * 512,
+        52,
+        (4, 5, 6),
     )
     count = NZ * NY
     rim = lax.ppermute(pool[ROWS - 16 :], SP, [(k, k + 1) for k in range(count - 1)])
-    heads = lax.all_to_all(msg.reshape(8, 128, 128), TP, 0, 0, tiled=True)
-    mine = lax.all_to_all(heads.reshape(16, 64, 128), "z", 0, 0, tiled=True)
-    kx = lax.all_gather(mine[:, 0:32], "x", axis=0, tiled=False)
-    ko = swap(kx)
+    heads = lax.all_to_all(msg.reshape(8, 112, 128), TP, 0, 0, tiled=True)
+    mine = lax.all_to_all(heads.reshape(16, 56, 128), "z", 0, 0, tiled=True)
+    ks = spread(mine[:, 0:32], TP)
     qy = lax.all_gather(mine[:, 32:48], "y", axis=0, tiled=False)
+    (pooled,) = call(
+        pool_kernel, (x, (z * NY + y) * ROWS), (rim, pool), [(ROWS, 128)], [], 2**20, 4
+    )
+    pools = spread(pooled, TP)
     (parts,) = call(
         attend_kernel,
-        "attend",
-        (y, c, 2 * x + c),
-        (kx, ko, qy, mine[:, 48:64]),
+        (y, 2 * x + c),
+        (ks, qy, mine[:, 48:56]),
         [(NY, 512, 128)],
         [
             pltpu.VMEM((4096, 128), BF16),
@@ -282,29 +302,22 @@
             pltpu.VMEM((9, 256, 512), F32),
         ],
         4 * 72 * 256 * 256 * 128,
-    )
+        24,
+    )
+    parts, pools = lax.optimization_barrier((parts, pools))
     parts = lax.all_to_all(parts, "y", 0, 0, tiled=True)
-    merged, pooled = call(
-        merge_kernel,
-        "merge",
-        (x, (z * NY + y) * ROWS),
-        (parts, rim, pool),
-        [(16, 16, 128), (ROWS, 128)],
-        [],
-        2**20,
-    )
+    (merged,) = call(merge_kernel, (c,), (parts,), [(16, 16, 128)], [], 2**20, 8)
     back = lax.all_to_all(merged, "z", 0, 0, tiled=True)
-    both = jnp.concatenate([back.reshape(256, 128), pooled], axis=0)
-    own = lax.all_gather(both, "x", axis=0, tiled=False)
+    own = lax.all_gather(back.reshape(256, 128), "x", axis=0, tiled=False)
     other = swap(own)
     (mixed,) = call(
         output_kernel,
-        "output",
         (c,),
-        (own, other, wpo, wao),
+        (own, other, pools, wpo, wao),
         [(ROWS, 256)],
         [pltpu.VMEM((ROWS, 1024), BF16), pltpu.VMEM((ROWS, 1024), BF16)],
         2 * ROWS * 2048 * 256,
+        12,
     )
     return mixed
 
@@ -312,7 +325,7 @@
 def solution(mesh):
     grid = Mesh(mesh.devices.reshape(NZ, NY, NX, NC), ("z", "y", "x", "c"))
     return jax.shard_map(
-        per_device,
+        layer,
         mesh=grid,
         in_specs=(
             P(SP, TP),

time: 160 us -> 163 us (1.019)
  waiting for transfers between devices: 6.52 us -> 13.7 us
  blocking collectives: 93.9 us -> 90.9 us
    all_gather x4 -> x3, blocking collectives: 42 us -> 31.5 us  [the longest x1 11.4 us: layer(): own = lax.all_gather(tokens, 'x', axis=0, tiled=False)]
    ppermute x3 -> x2, starting transfers between devices: 31.9 us -> 21.5 us  [swap(): return lax.ppermute(value, 'c', [(0, 1), (1, 0)])]
    all_to_all x1 -> x2, starting transfers between devices: 3.47 us -> 13.7 us  [spread(): return lax.all_to_all(copies, axis, 0, 0, tiled=True)]
    all_to_all x3 -> x4, blocking collectives: 51.9 us -> 59.4 us  [the longest x1 23.7 us: layer(): mine = lax.all_to_all(heads.reshape(16, 56, 128), 'z', 0, 0, tiled=True)]
    all_to_all x1 -> x2, waiting for transfers between devices: 2.83 us -> 10.4 us  [spread(): return lax.all_to_all(copies, axis, 0, 0, tiled=True)]
    unnamed x20 -> x14, local copies, waits for them, and re-layouts: 3.81 us -> 0.68 us
    broadcast_in_dim x0 -> x2, local copies, waits for them, and re-layouts: none -> 2.02 us  [spread(): copies = jnp.broadcast_to(value[None], (size, *value.shape))]
    pallas_call x4 -> x5, Pallas kernels: 16.5 us -> 16.7 us  [call(): pl.pallas_call(kernel, out_shape=shapes, in_specs=[SM] + [HB if k in in_h...]
  transfers between devices with their start and end apart: 5 -> 5, of which waited for: 4 -> 4; matrix products, arithmetic and copies ran while one was open for 0% -> 0% of each run, Pallas kernels for 0% -> 7%
where the time goes in v2:
time: 163 us
  blocking collectives  90.9 us (56%)
  starting transfers between devices  38.4 us (24%)
  Pallas kernels  16.7 us (10%)
  waiting for transfers between devices  13.7 us (8%)
  local copies, waits for them, and re-layouts  2.72 us (2%)
    all_to_all x1, blocking collectives, layer(): mine = lax.all_to_all(heads.reshape(16, 56, 128), 'z', 0, 0, tiled=True)  23.7 us
    ppermute x2, starting transfers between devices, swap(): return lax.ppermute(value, 'c', [(0, 1), (1, 0)])  21.5 us
    pallas_call x5, Pallas kernels, call(): pl.pallas_call(kernel, out_shape=shapes, in_specs=[SM] + [HB if k in in_h...  16.7 us
    all_to_all x1, blocking collectives, layer(): back = lax.all_to_all(merged, 'z', 0, 0, tiled=True)  16.4 us
    all_to_all x2, starting transfers between devices, spread(): return lax.all_to_all(copies, axis, 0, 0, tiled=True)  13.7 us
    all_gather x1, blocking collectives, layer(): own = lax.all_gather(tokens, 'x', axis=0, tiled=False)  11.4 us
    all_gather x1, blocking collectives, layer(): qy = lax.all_gather(mine[:, 32:48], 'y', axis=0, tiled=False)  10.4 us
    all_to_all x2, waiting for transfers between devices, spread(): return lax.all_to_all(copies, axis, 0, 0, tiled=True)  10.4 us
  transfers between devices with their start and end apart: 5, of which 4 were waited for; matrix products, arithmetic and copies ran while one was open for 0% of the time, Pallas kernels for 7%

profile of v2, /device:TPU:1, one launch (start us, length us, event | category | flops | bytes accessed | tf_op | source)
XLA Modules:
  0.0 162.7 jit_solution(10647125741756536928)
XLA Ops:
  0.0 11.4 %all-gather = bf16[1024,256]{1,0:T(8,128)(2,1)S(1)} all-gather(bf16[256,256]{1,0:T(8,128)(2,1)} %param.11), channel_id=2, replica_groups=mesh['z'=16,'y'=4,'x'=4,'c'=2] {'x'}, dimensions={0}, use_global_device_ids=true | all-gather | bytes 655360 | tf_op jit(solution)/shard_map/all_gather | solution.py:257
  11.4 10.6 %collective-permute-start = (bf16[4,256,256]{2,1,0:T(8,128)(2,1)S(1)}, bf16[4,256,256]{2,1,0:T(8,128)(2,1)S(1)}, u32[]{:S(2)}, u32[]{:S(2)}) collective-permute-start(bf16[4,256,256]{2,1,0:T(8,128)(2,1)S(1)} %bitcast.14), channel_id=1, source_target_pairs={{0,1},{1,0},{2,3},{3,2},{4,5},{5,4},{6,7},{7,6},{8,9},{9,8},{10,11... | collective-permute-start | bytes 1572872 | tf_op jit(solution)/shard_map/ppermute | solution.py:250
  22.0 1.5 collective-permute-done.other
  23.5 0.0 copy-done.2
  23.5 0.0 copy-done.3
  23.5 0.7 copy-done.4
  24.2 0.0 copy-done.5
  24.2 0.0 copy-done.6
  24.2 3.4 %shard_map.109 = (bf16[8,2,56,128]{3,2,1,0:T(8,128)(2,1)S(1)}, bf16[256,128]{1,0:T(8,128)(2,1)S(1)}) custom-call(s32[1]{0:T(128)} %bitcast.where, bf16[4,256,256]{2,1,0:T(8,128)(2,1)S(1)} %bitcast.15, bf16[4,256,256]{2,1,0:T(8,128)(2,1)S(1)} %collective-permute-done.other, f32[1,2048]{1,0:T(1,128)S(1)} %bitcast.18, bf16[128,2048]{1,0:T(8,128)(2,1)S(1)} %copy-done.2, ...), custom_call_target="tpu_custom_call" | custom-call | flops 536870912 | bytes 1048576 | tf_op jit(solution)/shard_map/pallas_call | solution.py:232
  27.6 9.1 %all_to_all.30 = bf16[8,112,128]{2,1,0:T(8,128)(2,1)S(1)} all-to-all(bf16[8,112,128]{2,1,0:T(8,128)(2,1)S(1)} %bitcast.17), channel_id=1, replica_groups=mesh['z'=16,'y'=4,'x'=4,'c'=2] {'x','c'}, dimensions={0} | all-to-all | bytes 458752 | tf_op jit(solution)/shard_map/all_to_all | solution.py:284
  36.7 23.7 %all_to_all.31 = bf16[16,56,128]{2,1,0:T(8,128)(2,1)S(1)} all-to-all(bf16[16,56,128]{2,1,0:T(8,128)(2,1)S(1)} %bitcast.22), channel_id=1, replica_groups=mesh['z'=16,'y'=4,'x'=4,'c'=2] {'z'}, dimensions={0} | all-to-all | bytes 458752 | tf_op jit(solution)/shard_map/all_to_all | solution.py:285
  60.4 1.2 broadcast_in_dim.4
  61.6 9.4 %all-to-all-start.2 = ((bf16[8,16,32,128]{3,2,1,0:T(8,128)(2,1)}), bf16[8,16,32,128]{3,2,1,0:T(8,128)(2,1)S(1)}, u32[]{:S(2)}, u32[]{:S(2)}) async-start(bf16[8,16,32,128]{3,2,1,0:T(8,128)(2,1)} %broadcast_in_dim.4), calls=%async_computation.2 | async-start | bytes 2097152 | tf_op jit(solution)/shard_map/all_to_all | solution.py:246
  70.9 3.2 %collective-permute-start.1 = (bf16[16,128]{1,0:T(8,128)(2,1)S(1)}, bf16[16,128]{1,0:T(8,128)(2,1)S(1)}, u32[]{:S(2)}, u32[]{:S(2)}) collective-permute-start(bf16[16,128]{1,0:T(8,128)(2,1)S(1)} %slice.15), channel_id=1, source_target_pairs={{0,8},{8,16},{16,24},{24,32},{32,40},{40,48},{48,56},{56,64},{64,7... | collective-permute-start | bytes 12296 | tf_op jit(solution)/shard_map/ppermute | solution.py:283
  74.1 0.1 pad_add_fusion.1.where
  74.2 0.7 collective-permute-done.1.rim
  74.9 0.7 shard_map.111
  75.6 10.4 %all-to-all-done.2.ks = bf16[8,16,32,128]{3,2,1,0:T(8,128)(2,1)S(1)} async-done(((bf16[8,16,32,128]{3,2,1,0:T(8,128)(2,1)}), bf16[8,16,32,128]{3,2,1,0:T(8,128)(2,1)S(1)}, u32[]{:S(2)}, u32[]{:S(2)}) %all-to-all-start.2) | async-done | bytes 1048608 | tf_op jit(solution)/shard_map/all_to_all | solution.py:246
  85.9 0.9 broadcast_in_dim.5
  86.8 4.4 %all-to-all-start.3 = ((bf16[8,256,128]{2,1,0:T(8,128)(2,1)}), bf16[8,256,128]{2,1,0:T(8,128)(2,1)S(1)}, u32[]{:S(2)}, u32[]{:S(2)}) async-start(bf16[8,256,128]{2,1,0:T(8,128)(2,1)} %broadcast_in_dim.5), calls=%async_computation.3 | async-start | bytes 1048576 | tf_op jit(solution)/shard_map/all_to_all | solution.py:246
  91.2 0.1 pad_add_fusion.where
  91.2 10.4 %all-gather.1 = bf16[64,16,128]{2,1,0:T(8,128)(2,1)S(1)} all-gather(bf16[16,16,128]{2,1,0:T(8,128)(2,1)S(1)} %slice.17), channel_id=3, replica_groups=mesh['z'=16,'y'=4,'x'=4,'c'=2] {'y'}, dimensions={0}, use_global_device_ids=true | all-gather | bytes 327680 | tf_op jit(solution)/shard_map/all_gather | solution.py:287
  101.6 10.8 %shard_map.110 = bf16[4,512,128]{2,1,0:T(8,128)(2,1)S(1)} custom-call(s32[2]{0:T(128)S(1)} %pad_add_fusion.where, bf16[8,16,32,128]{3,2,1,0:T(8,128)(2,1)S(1)} %all-to-all-done.2.ks, bf16[4,16,16,128]{3,2,1,0:T(8,128)(2,1)S(1)} %bitcast.16, bf16[16,8,128]{2,1,0:T(8,128)(2,1)S(1)} %slice.18.gates), custom_call_target="tpu_custom_call" | custom-call | flops 2415919104 | bytes 1048576 | tf_op jit(solution)/shard_map/pallas_call | solution.py:232
  112.4 0.0 all-to-all-done.3.pools
  112.4 10.2 %all_to_all.32.parts = bf16[4,512,128]{2,1,0:T(8,128)(2,1)S(1)} all-to-all(bf16[4,512,128]{2,1,0:T(8,128)(2,1)S(1)} %shard_map.110), channel_id=1, replica_groups=mesh['z'=16,'y'=4,'x'=4,'c'=2] {'y'}, dimensions={0} | all-to-all | bytes 1048576 | tf_op jit(solution)/shard_map/all_to_all | solution.py:308
  122.6 0.6 shard_map.112
  123.2 16.4 %all_to_all.33 = bf16[16,16,128]{2,1,0:T(8,128)(2,1)S(1)} all-to-all(bf16[16,16,128]{2,1,0:T(8,128)(2,1)S(1)} %shard_map.112), channel_id=1, replica_groups=mesh['z'=16,'y'=4,'x'=4,'c'=2] {'z'}, dimensions={0} | all-to-all | bytes 131072 | tf_op jit(solution)/shard_map/all_to_all | solution.py:310
  139.6 9.7 %all_gather.19.own = bf16[4,256,128]{2,1,0:T(8,128)(2,1)S(1)} all-gather(bf16[1,256,128]{2,1,0:T(8,128)(2,1)S(1)} %bitcast.23), channel_id=1, replica_groups=mesh['z'=16,'y'=4,'x'=4,'c'=2] {'x'}, dimensions={0}, use_global_device_ids=true | all-gather | bytes 327680 | tf_op jit(solution)/shard_map/all_gather | solution.py:311
  149.3 10.9 %collective-permute-start.2 = (bf16[4,256,128]{2,1,0:T(8,128)(2,1)S(1)}, bf16[4,256,128]{2,1,0:T(8,128)(2,1)S(1)}, u32[]{:S(2)}, u32[]{:S(2)}) collective-permute-start(bf16[4,256,128]{2,1,0:T(8,128)(2,1)S(1)} %all_gather.19.own), channel_id=1, source_target_pairs={{0,1},{1,0},{2,3},{3,2},{4,5},{5,4},{6,7},{7,6},{8,9},{9,8},{10,11... | collective-permute-start | bytes 786440 | tf_op jit(solution)/shard_map/ppermute | solution.py:250
  160.3 1.1 collective-permute-done.2.other
  161.4 0.0 copy-done
  161.4 1.3 shard_map.113
  (12 shorter events, 0.0 us)
Async XLA Ops:
  0.0 23.5 %copy-start.2 = (bf16[128,2048]{1,0:T(8,128)(2,1)S(1)}, bf16[128,2048]{1,0:T(8,128)(2,1)}, u32[]{:S(2)}) copy-start(bf16[128,2048]{1,0:T(8,128)(2,1)} %wq.1) | copy-start | bytes 1572868
  11.4 12.1 %copy-start.3 = (f32[2048]{0:T(1024)S(1)}, f32[2048]{0:T(1024)}, u32[]{:S(2)}) copy-start(f32[2048]{0:T(1024)} %param.12) | copy-start | bytes 24580
  11.4 12.1 %collective-permute-start = (bf16[4,256,256]{2,1,0:T(8,128)(2,1)S(1)}, bf16[4,256,256]{2,1,0:T(8,128)(2,1)S(1)}, u32[]{:S(2)}, u32[]{:S(2)}) collective-permute-start(bf16[4,256,256]{2,1,0:T(8,128)(2,1)S(1)} %bitcast.14), channel_id=1, source_target_pairs={{0,1},{1,0},{2,3},{3,2},{4,5},{5,4},{6,7},{7,6},{8,9},{9,8},{10,11... | collective-permute-start | bytes 1572872 | tf_op jit(solution)/shard_map/ppermute | solution.py:250
  23.5 0.7 copy-start.4
  23.5 0.7 copy-start.5
  23.5 0.7 copy-start.6
  61.6 24.4 %all-to-all-start.2 = ((bf16[8,16,32,128]{3,2,1,0:T(8,128)(2,1)}), bf16[8,16,32,128]{3,2,1,0:T(8,128)(2,1)S(1)}, u32[]{:S(2)}, u32[]{:S(2)}) async-start(bf16[8,16,32,128]{3,2,1,0:T(8,128)(2,1)} %broadcast_in_dim.4), calls=%async_computation.2 | async-start | bytes 2097152 | tf_op jit(solution)/shard_map/all_to_all | solution.py:246
  70.9 3.9 %collective-permute-start.1 = (bf16[16,128]{1,0:T(8,128)(2,1)S(1)}, bf16[16,128]{1,0:T(8,128)(2,1)S(1)}, u32[]{:S(2)}, u32[]{:S(2)}) collective-permute-start(bf16[16,128]{1,0:T(8,128)(2,1)S(1)} %slice.15), channel_id=1, source_target_pairs={{0,8},{8,16},{16,24},{24,32},{32,40},{40,48},{48,56},{56,64},{64,7... | collective-permute-start | bytes 12296 | tf_op jit(solution)/shard_map/ppermute | solution.py:283
  86.8 25.6 %all-to-all-start.3 = ((bf16[8,256,128]{2,1,0:T(8,128)(2,1)}), bf16[8,256,128]{2,1,0:T(8,128)(2,1)S(1)}, u32[]{:S(2)}, u32[]{:S(2)}) async-start(bf16[8,256,128]{2,1,0:T(8,128)(2,1)} %broadcast_in_dim.5), calls=%async_computation.3 | async-start | bytes 1048576 | tf_op jit(solution)/shard_map/all_to_all | solution.py:246
  122.6 38.8 %copy-start = (bf16[1024,256]{1,0:T(8,128)(2,1)S(1)}, bf16[1024,256]{1,0:T(8,128)(2,1)}, u32[]{:S(2)}) copy-start(bf16[1024,256]{1,0:T(8,128)(2,1)} %wpo.1) | copy-start | bytes 1572868
  122.6 38.8 %copy-start.1 = (bf16[1024,256]{1,0:T(8,128)(2,1)S(1)}, bf16[1024,256]{1,0:T(8,128)(2,1)}, u32[]{:S(2)}) copy-start(bf16[1024,256]{1,0:T(8,128)(2,1)} %wao.1) | copy-start | bytes 1572868
  149.3 12.1 %collective-permute-start.2 = (bf16[4,256,128]{2,1,0:T(8,128)(2,1)S(1)}, bf16[4,256,128]{2,1,0:T(8,128)(2,1)S(1)}, u32[]{:S(2)}, u32[]{:S(2)}) collective-permute-start(bf16[4,256,128]{2,1,0:T(8,128)(2,1)S(1)} %all_gather.19.own), channel_id=1, source_target_pairs={{0,1},{1,0},{2,3},{3,2},{4,5},{5,4},{6,7},{7,6},{8,9},{9,8},{10,11... | collective-permute-start | bytes 786440 | tf_op jit(solution)/shard_map/ppermute | solution.py:250

commit v3 on v2

--- a/solution.py
+++ b/solution.py
@@ -73,8 +73,11 @@
     for h in range(2):
         kv = jnp.concatenate([k[h], v[:, h * HEAD : (h + 1) * HEAD]], axis=-1).astype(BF16)
         g = three_parts(gate[h : h + 1, :])
-        lines = [g[i][:, 128 * j : 128 * (j + 1)] for i in range(3) for j in range(2)]
-        lines = jnp.concatenate(lines + [jnp.zeros((2, 128), F32)], axis=0).astype(BF16)
+        zero = jnp.zeros((1, 128), F32)
+        lines = []
+        for j in range(2):
+            lines += [v[:, 128 * j : 128 * (j + 1)] for v in g] + [zero]
+        lines = jnp.concatenate(lines, axis=0).astype(BF16)
         for s in range(8):
             msg[s, h, 0:32, :] = kv[32 * s : 32 * s + 32]
             a = q[h][32 * s : 32 * s + 16]
@@ -83,45 +86,47 @@
             msg[s, h, 48:56, :] = lines
 
 
-def attend_kernel(where, ks, qy, gates, out, kv, qs, bias, gap, buf):
+def attend_kernel(where, ks, qy, gates, out, kv, vt, qs, gap, buf, lse):
     y, s = where[0], where[1]
     lane = iota((16, 128), 1)
     for z in range(NZ):
         for k in range(8):
-            kv[z * 256 + 32 * k : z * 256 + 32 * k + 32, :] = ks[k, z]
-        g = gates[z].astype(F32)
-        g = g[0:2] + g[2:4] + g[4:6]
+            kv[z * 256 + 32 * k : z * 256 + 32 * k + 32, 0:128] = ks[k, z]
+        g = gates[z].astype(F32).T
+        pad = jnp.zeros((128, 120), F32)
         for j in range(2):
-            at = (z % 2) * 256 + j * 128
-            bias[z // 2, :, at : at + 128] = jnp.broadcast_to(g[j : j + 1], (8, 128))
+            part = jnp.where(iota((128, 8), 1) // 4 == j, g, 0.0)
+            at = z * 256 + 128 * j
+            kv[at : at + 128, 128:256] = jnp.concatenate([part, pad], axis=1).astype(BF16)
+            vt[:, at : at + 128] = kv[at : at + 128, 0:128].T[64:128]
         for yy in range(NY):
             p = qy[yy, z].astype(F32)
-            base = yy * 64 + (z % 2) * 32
-            qs[z // 2, base : base + 16, :] = jnp.where(lane < 64, p, 0.0).astype(BF16)
-            qs[z // 2, base + 16 : base + 32, :] = jnp.where(
-                lane < 64, pltpu.roll(p, 64, 1), 0.0
-            ).astype(BF16)
-    r = iota((256, 512), 0)
-    l = iota((256, 512), 1)
-    q_at = (((r // 32) % 2) * 4 + r // 64) * 256 + 32 * s + r % 32
-    k_at = ((l // 256) * 4 + y) * 256 + l % 256
+            for half in range(2):
+                base = half * 128 + yy * 32 + (z % 2) * 16
+                q = p if half == 0 else pltpu.roll(p, 64, 1)
+                qs[z // 2, base : base + 16, 0:128] = jnp.where(lane < 64, q, 0.0).astype(BF16)
+    ln = iota((256, 128), 1)
+    signs = jnp.where((ln < 7) & (ln != 3), -1.0, 0.0).astype(BF16)
+    for m in range(8):
+        qs[m, :, 128:256] = signs
+    r = iota((512, 256), 0)
+    l = iota((512, 256), 1)
+    k_at = ((r // 256) * 4 + y) * 256 + r % 256
+    q_at = (((l // 16) % 2) * 4 + (l // 32) % 4) * 256 + 32 * s + (l // 128) * 16 + l % 16
     gap[...] = k_at - q_at
 
     def step(i, carry):
-        low = jnp.full((256, 128), NEG, F32)
+        low = jnp.full((8, 256), NEG, F32)
         tops = [low, low]
         for t in range(9):
             first = t <= i
             qi = jnp.where(first, i, 7 - i)
             j = jnp.where(first, t, t - i - 1)
             keys = kv[pl.ds(pl.multiple_of(j * 512, 512), 512), :]
-            logits = dot_t(qs[qi], keys) - bias[j, 0:1, :]
+            logits = dot_t(keys, qs[qi])
             logits = jnp.where(gap[...] <= 2048 * (qi - j), logits, NEG)
             buf[t] = logits
-            m = jnp.maximum(
-                jnp.maximum(logits[:, 0:128], logits[:, 128:256]),
-                jnp.maximum(logits[:, 256:384], logits[:, 384:512]),
-            )
+            m = jnp.max(logits.reshape(64, 8, 256), axis=0)
             if t == 0:
                 tops[0] = m
             elif t >= 4:
@@ -129,13 +134,12 @@
             else:
                 tops[0] = jnp.where(first, jnp.maximum(tops[0], m), tops[0])
                 tops[1] = jnp.where(first, tops[1], jnp.maximum(tops[1], m))
-        tops = [jnp.maximum(jnp.max(m, axis=-1, keepdims=True), -1e29) for m in tops]
-        zero = jnp.zeros((256, 128), F32)
-        sums, accs = [zero, zero], [zero, zero]
+        tops = [jnp.maximum(jnp.max(m, axis=0, keepdims=True), -1e29) for m in tops]
+        sums = [jnp.zeros((8, 256), F32)] * 2
+        accs = [jnp.zeros((64, 256), F32)] * 2
         for t in range(9):
             first = t <= i
             j = jnp.where(first, t, t - i - 1)
-            keys = kv[pl.ds(pl.multiple_of(j * 512, 512), 512), :]
             if t == 0:
                 m = tops[0]
             elif t >= 4:
@@ -143,8 +147,8 @@
             else:
                 m = jnp.where(first, tops[0], tops[1])
             w = jnp.exp(buf[t] - m)
-            n = (w[:, 0:128] + w[:, 128:256]) + (w[:, 256:384] + w[:, 384:512])
-            a = dot(w.astype(BF16), keys)
+            n = jnp.sum(w.reshape(64, 8, 256), axis=0)
+            a = dot(vt[:, pl.ds(pl.multiple_of(j * 512, 512), 512)], w.astype(BF16))
             if t == 0:
                 sums[0], accs[0] = n, a
             elif t >= 4:
@@ -154,36 +158,46 @@
                 accs[0] = jnp.where(first, accs[0] + a, accs[0])
                 sums[1] = jnp.where(first, sums[1], sums[1] + n)
                 accs[1] = jnp.where(first, accs[1], accs[1] + a)
-        ln = iota((256, 128), 1)
         for k in range(2):
-            n = jnp.sum(sums[k], axis=-1, keepdims=True)
+            n = jnp.sum(sums[k], axis=0, keepdims=True)
             some = n > 0.0
             safe = jnp.where(some, n, 1.0)
-            o = pltpu.roll(accs[k] / safe, 64, 1)
-            p0, p1, p2 = three_parts(jnp.where(some, tops[k] + jnp.log(safe), NEG))
-            tail = jnp.where(ln == 64, p0, jnp.where(ln == 65, p1, p2))
-            o = jnp.where(ln < 64, o, jnp.where(ln < 67, tail, 0.0)).astype(BF16)
             m = i if k == 0 else 7 - i
+            lse[pl.ds(m, 1), :] = jnp.where(some, tops[k] + jnp.log(safe), NEG)
+            o = accs[k] / safe
+            o = jnp.concatenate([o[:, 0:128], o[:, 128:256]], axis=0).T.astype(BF16)
             for yy in range(NY):
-                out[yy, pl.ds(pl.multiple_of(m * 64, 64), 64), :] = o[64 * yy : 64 * yy + 64]
+                at = pl.multiple_of(m * 32, 32)
+                out[yy, pl.ds(at, 32), :] = o[32 * yy : 32 * yy + 32]
         return carry
 
     lax.fori_loop(0, 4, step, 0)
+    ln = iota((8, 128), 1)
+    for yy in range(NY):
+        a = pltpu.roll(lse[:, 0:128], (128 - 32 * yy) % 128, 1)
+        b = pltpu.roll(lse[:, 128:256], (160 - 32 * yy) % 128, 1)
+        v = jnp.where(ln < 32, a, jnp.where(ln < 64, b, 0.0))
+        out[yy, 256:280, :] = jnp.concatenate(three_parts(v), axis=0).astype(BF16)
 
 
 def merge_kernel(where, parts, out):
-    vals = [parts[k].astype(F32) for k in range(NY)]
-    ln = iota((512, 128), 1)
-    stat = (ln >= 64) & (ln < 67)
-    lses = [jnp.sum(jnp.where(stat, v, 0.0), axis=-1, keepdims=True) for v in vals]
+    lses = []
+    for k in range(NY):
+        v = parts[k, 256:280, :].astype(F32)
+        lses.append(v[0:8] + v[8:16] + v[16:24])
     top = jnp.maximum(jnp.maximum(lses[0], lses[1]), jnp.maximum(lses[2], lses[3]))
     ws = [jnp.exp(v - top) for v in lses]
     den = (ws[0] + ws[1]) + (ws[2] + ws[3])
-    o = (ws[0] * vals[0] + ws[1] * vals[1] + ws[2] * vals[2] + ws[3] * vals[3]) / den
-    o = o.reshape(16, 2, 16, 128)
-    half = iota((16, 16, 128), 2) < 64
-    back = pltpu.roll(o[:, 1].reshape(256, 128), 64, 1).reshape(16, 16, 128)
-    out[...] = jnp.where(half, o[:, 0], back).astype(BF16)
+    ws = [(w / den).T for w in ws]
+    half = iota((16, 128), 1) < 64
+    for z in range(NZ):
+        m, at = z // 2, (z % 2) * 16
+        total = jnp.zeros((16, 128), F32)
+        for k in range(NY):
+            a = ws[k][at : at + 16, m : m + 1]
+            b = ws[k][at + 32 : at + 48, m : m + 1]
+            total = total + jnp.where(half, a, b) * parts[k, 16 * z : 16 * z + 16, :].astype(F32)
+        out[z] = total.astype(BF16)
 
 
 def pool_kernel(where, rim, cur, pooled):
@@ -202,13 +216,13 @@
     pooled[...] = (mean - now).astype(BF16)
 
 
-def output_kernel(where, own, other, pools, wpo, wao, out, pooled, attended):
+def output_kernel(where, own, other, wpo, wao, out, pooled, attended):
     c = where[0]
     half = iota((16, 128), 1) < 64
     for x in range(NX):
         for k, ref in enumerate((own, other)):
             s = 2 * x + (c if k == 0 else 1 - c)
-            pooled[:, 128 * (2 * x + k) : 128 * (2 * x + k + 1)] = pools[2 * x + k]
+            pooled[:, pl.ds(pl.multiple_of(s * 128, 128), 128)] = ref[x, 256:512, :]
             for j in range(8):
                 a = ref[x, 32 * j : 32 * j + 16, :].astype(F32)
                 b = ref[x, 32 * j + 16 : 32 * j + 32, :].astype(F32)
@@ -280,40 +294,40 @@
         (4, 5, 6),
     )
     count = NZ * NY
-    rim = lax.ppermute(pool[ROWS - 16 :], SP, [(k, k + 1) for k in range(count - 1)])
     heads = lax.all_to_all(msg.reshape(8, 112, 128), TP, 0, 0, tiled=True)
     mine = lax.all_to_all(heads.reshape(16, 56, 128), "z", 0, 0, tiled=True)
     ks = spread(mine[:, 0:32], TP)
     qy = lax.all_gather(mine[:, 32:48], "y", axis=0, tiled=False)
-    (pooled,) = call(
-        pool_kernel, (x, (z * NY + y) * ROWS), (rim, pool), [(ROWS, 128)], [], 2**20, 4
-    )
-    pools = spread(pooled, TP)
     (parts,) = call(
         attend_kernel,
         (y, 2 * x + c),
         (ks, qy, mine[:, 48:56]),
-        [(NY, 512, 128)],
+        [(NY, 280, 128)],
         [
-            pltpu.VMEM((4096, 128), BF16),
-            pltpu.VMEM((8, 256, 128), BF16),
-            pltpu.VMEM((8, 8, 512), F32),
-            pltpu.VMEM((256, 512), jnp.int32),
-            pltpu.VMEM((9, 256, 512), F32),
+            pltpu.VMEM((4096, 256), BF16),
+            pltpu.VMEM((64, 4096), BF16),
+            pltpu.VMEM((8, 256, 256), BF16),
+            pltpu.VMEM((512, 256), jnp.int32),
+            pltpu.VMEM((9, 512, 256), F32),
+            pltpu.VMEM((8, 256), F32),
         ],
         4 * 72 * 256 * 256 * 128,
         24,
     )
-    parts, pools = lax.optimization_barrier((parts, pools))
     parts = lax.all_to_all(parts, "y", 0, 0, tiled=True)
     (merged,) = call(merge_kernel, (c,), (parts,), [(16, 16, 128)], [], 2**20, 8)
+    rim = lax.ppermute(pool[ROWS - 16 :], SP, [(k, k + 1) for k in range(count - 1)])
+    (pooled,) = call(
+        pool_kernel, (x, (z * NY + y) * ROWS), (rim, pool), [(ROWS, 128)], [], 2**20, 4
+    )
     back = lax.all_to_all(merged, "z", 0, 0, tiled=True)
-    own = lax.all_gather(back.reshape(256, 128), "x", axis=0, tiled=False)
+    both = jnp.concatenate([back.reshape(256, 128), pooled], axis=0)
+    own = lax.all_gather(both, "x", axis=0, tiled=False)
     other = swap(own)
     (mixed,) = call(
         output_kernel,
         (c,),
-        (own, other, pools, wpo, wao),
+        (own, other, wpo, wao),
         [(ROWS, 256)],
         [pltpu.VMEM((ROWS, 1024), BF16), pltpu.VMEM((ROWS, 1024), BF16)],
         2 * ROWS * 2048 * 256,

time: 163 us -> 147 us (0.902)
  blocking collectives: 90.9 us -> 74.7 us
  starting transfers between devices: 38.4 us -> 35.9 us
  waiting for transfers between devices: 13.7 us -> 15.7 us
    all_to_all x1 -> x0, blocking collectives: 16.4 us -> none  [layer(): back = lax.all_to_all(merged, 'z', 0, 0, tiled=True)]
    all_to_all x0 -> x1, waiting for transfers between devices: none -> 7.92 us  [layer(): back = lax.all_to_all(merged, 'z', 0, 0, tiled=True)]
    all_to_all x2 -> x1, waiting for transfers between devices: 10.4 us -> 4.13 us  [spread(): return lax.all_to_all(copies, axis, 0, 0, tiled=True)]
    all_to_all x0 -> x1, starting transfers between devices: none -> 5.01 us  [layer(): back = lax.all_to_all(merged, 'z', 0, 0, tiled=True)]
    all_to_all x2 -> x1, starting transfers between devices: 13.7 us -> 9.36 us  [spread(): return lax.all_to_all(copies, axis, 0, 0, tiled=True)]
    ppermute x2, starting transfers between devices: 21.5 us -> 19.3 us  [swap(): return lax.ppermute(value, 'c', [(0, 1), (1, 0)])]
  transfers between devices with their start and end apart: 5 -> 5, of which waited for: 4 -> 5; matrix products, arithmetic and copies ran while one was open for 0% -> 0% of each run, Pallas kernels for 7% -> 0%
where the time goes in v3:
time: 147 us; the launch traced here: 146 us
  blocking collectives  74.7 us (51%)
  starting transfers between devices  35.9 us (24%)
  Pallas kernels  17.7 us (12%)
  waiting for transfers between devices  15.7 us (11%)
  local copies, waits for them, and re-layouts  1.87 us (1%)
    all_to_all x1, blocking collectives, layer(): mine = lax.all_to_all(heads.reshape(16, 56, 128), 'z', 0, 0, tiled=True)  23.7 us
    ppermute x2, starting transfers between devices, swap(): return lax.ppermute(value, 'c', [(0, 1), (1, 0)])  19.3 us
    pallas_call x5, Pallas kernels, call(): pl.pallas_call(kernel, out_shape=shapes, in_specs=[SM] + [HB if k in in_h...  17.7 us
    all_gather x1, blocking collectives, layer(): own = lax.all_gather(tokens, 'x', axis=0, tiled=False)  11.4 us
    all_gather x1, blocking collectives, layer(): qy = lax.all_gather(mine[:, 32:48], 'y', axis=0, tiled=False)  10.8 us
    all_gather x1, blocking collectives, layer(): own = lax.all_gather(both, 'x', axis=0, tiled=False)  10.1 us
    all_to_all x1, blocking collectives, layer(): parts = lax.all_to_all(parts, 'y', 0, 0, tiled=True)  9.65 us
    all_to_all x1, starting transfers between devices, spread(): return lax.all_to_all(copies, axis, 0, 0, tiled=True)  9.36 us
  transfers between devices with their start and end apart: 5, of which 5 were waited for; matrix products, arithmetic and copies ran while one was open for 0% of the time, Pallas kernels for 0%

profile of v3, /device:TPU:1, one launch (start us, length us, event | category | flops | bytes accessed | tf_op | source)
XLA Modules:
  0.0 146.2 jit_solution(10157460834433319159)
XLA Ops:
  0.0 0.0 copy-start.2
  0.0 11.4 %all-gather = bf16[1024,256]{1,0:T(8,128)(2,1)S(1)} all-gather(bf16[256,256]{1,0:T(8,128)(2,1)} %param.11), channel_id=2, replica_groups=mesh['z'=16,'y'=4,'x'=4,'c'=2] {'x'}, dimensions={0}, use_global_device_ids=true | all-gather | bytes 655360 | tf_op jit(solution)/shard_map/all_gather | solution.py:271
  11.4 10.6 %collective-permute-start = (bf16[4,256,256]{2,1,0:T(8,128)(2,1)S(1)}, bf16[4,256,256]{2,1,0:T(8,128)(2,1)S(1)}, u32[]{:S(2)}, u32[]{:S(2)}) collective-permute-start(bf16[4,256,256]{2,1,0:T(8,128)(2,1)S(1)} %bitcast.17), channel_id=1, source_target_pairs={{0,1},{1,0},{2,3},{3,2},{4,5},{5,4},{6,7},{7,6},{8,9},{9,8},{10,11... | collective-permute-start | bytes 1572872 | tf_op jit(solution)/shard_map/ppermute | solution.py:264
  22.0 1.5 %collective-permute-done.other = bf16[4,256,256]{2,1,0:T(8,128)(2,1)S(1)} collective-permute-done((bf16[4,256,256]{2,1,0:T(8,128)(2,1)S(1)}, bf16[4,256,256]{2,1,0:T(8,128)(2,1)S(1)}, u32[]{:S(2)}, u32[]{:S(2)}) %collective-permute-start) | collective-permute-done | bytes 524320 | tf_op jit(solution)/shard_map/ppermute | solution.py:264
  23.5 0.0 copy-done.2
  23.5 0.0 copy-done.3
  23.5 0.7 copy-done.4
  24.2 0.0 copy-done.5
  24.2 0.0 copy-done.6
  24.2 3.4 %shard_map.109 = (bf16[8,2,56,128]{3,2,1,0:T(8,128)(2,1)S(1)}, bf16[256,128]{1,0:T(8,128)(2,1)S(1)}) custom-call(s32[1]{0:T(128)} %bitcast.where, bf16[4,256,256]{2,1,0:T(8,128)(2,1)S(1)} %bitcast.18, bf16[4,256,256]{2,1,0:T(8,128)(2,1)S(1)} %collective-permute-done.other, f32[1,2048]{1,0:T(1,128)S(1)} %bitcast.21, bf16[128,2048]{1,0:T(8,128)(2,1)S(1)} %copy-done.2, ...), custom_call_target="tpu_custom_call" | custom-call | flops 536870912 | bytes 1048576 | tf_op jit(solution)/shard_map/pallas_call | solution.py:246
  27.6 9.1 %all_to_all.25 = bf16[8,112,128]{2,1,0:T(8,128)(2,1)S(1)} all-to-all(bf16[8,112,128]{2,1,0:T(8,128)(2,1)S(1)} %bitcast.20), channel_id=1, replica_groups=mesh['z'=16,'y'=4,'x'=4,'c'=2] {'x','c'}, dimensions={0} | all-to-all | bytes 458752 | tf_op jit(solution)/shard_map/all_to_all | solution.py:297
  36.7 23.7 %all_to_all.26 = bf16[16,56,128]{2,1,0:T(8,128)(2,1)S(1)} all-to-all(bf16[16,56,128]{2,1,0:T(8,128)(2,1)S(1)} %bitcast.25), channel_id=1, replica_groups=mesh['z'=16,'y'=4,'x'=4,'c'=2] {'z'}, dimensions={0} | all-to-all | bytes 458752 | tf_op jit(solution)/shard_map/all_to_all | solution.py:298
  60.4 1.2 broadcast_in_dim.2
  61.6 9.4 %all-to-all-start.2 = ((bf16[8,16,32,128]{3,2,1,0:T(8,128)(2,1)}), bf16[8,16,32,128]{3,2,1,0:T(8,128)(2,1)S(1)}, u32[]{:S(2)}, u32[]{:S(2)}) async-start(bf16[8,16,32,128]{3,2,1,0:T(8,128)(2,1)} %broadcast_in_dim.2), calls=%async_computation.2 | async-start | bytes 2097152 | tf_op jit(solution)/shard_map/all_to_all | solution.py:260
  70.9 0.1 pad_add_fusion.where
  71.0 10.8 %all-gather.1 = bf16[64,16,128]{2,1,0:T(8,128)(2,1)S(1)} all-gather(bf16[16,16,128]{2,1,0:T(8,128)(2,1)S(1)} %slice.17), channel_id=3, replica_groups=mesh['z'=16,'y'=4,'x'=4,'c'=2] {'y'}, dimensions={0}, use_global_device_ids=true | all-gather | bytes 327680 | tf_op jit(solution)/shard_map/all_gather | solution.py:300
  81.8 4.1 %all-to-all-done.2.ks = bf16[8,16,32,128]{3,2,1,0:T(8,128)(2,1)S(1)} async-done(((bf16[8,16,32,128]{3,2,1,0:T(8,128)(2,1)}), bf16[8,16,32,128]{3,2,1,0:T(8,128)(2,1)S(1)}, u32[]{:S(2)}, u32[]{:S(2)}) %all-to-all-start.2) | async-done | bytes 1048608 | tf_op jit(solution)/shard_map/all_to_all | solution.py:260
  85.9 11.1 %shard_map.110 = bf16[4,280,128]{2,1,0:T(8,128)(2,1)S(1)} custom-call(s32[2]{0:T(128)S(1)} %pad_add_fusion.where, bf16[8,16,32,128]{3,2,1,0:T(8,128)(2,1)S(1)} %all-to-all-done.2.ks, bf16[4,16,16,128]{3,2,1,0:T(8,128)(2,1)S(1)} %bitcast.19, bf16[16,8,128]{2,1,0:T(8,128)(2,1)S(1)} %slice.18.gates), custom_call_target="tpu_custom_call" | custom-call | flops 2415919104 | bytes 1048576 | tf_op jit(solution)/shard_map/pallas_call | solution.py:246
  97.0 9.7 %all_to_all.27.parts = bf16[4,280,128]{2,1,0:T(8,128)(2,1)S(1)} all-to-all(bf16[4,280,128]{2,1,0:T(8,128)(2,1)S(1)} %shard_map.110), channel_id=1, replica_groups=mesh['z'=16,'y'=4,'x'=4,'c'=2] {'y'}, dimensions={0} | all-to-all | bytes 573440 | tf_op jit(solution)/shard_map/all_to_all | solution.py:317
  106.7 1.1 shard_map.111
  107.8 5.0 %all-to-all-start.4 = ((bf16[16,16,128]{2,1,0:T(8,128)(2,1)}), bf16[16,16,128]{2,1,0:T(8,128)(2,1)S(1)}, u32[]{:S(2)}, u32[]{:S(2)}) async-start(bf16[16,16,128]{2,1,0:T(8,128)(2,1)} %shard_map.111), calls=%async_computation.4 | async-start | bytes 131072 | tf_op jit(solution)/shard_map/all_to_all | solution.py:323
  112.8 2.2 %collective-permute-start.1 = (bf16[16,128]{1,0:T(8,128)(2,1)S(1)}, bf16[16,128]{1,0:T(8,128)(2,1)S(1)}, u32[]{:S(2)}, u32[]{:S(2)}) collective-permute-start(bf16[16,128]{1,0:T(8,128)(2,1)S(1)} %slice.15), channel_id=1, source_target_pairs={{0,8},{8,16},{16,24},{24,32},{32,40},{40,48},{48,56},{56,64},{64,7... | collective-permute-start | bytes 12296 | tf_op jit(solution)/shard_map/ppermute | solution.py:319
  115.0 0.1 pad_add_fusion.1.where
  115.1 0.7 collective-permute-done.1.rim
  115.8 0.7 shard_map.112
  116.5 7.9 %all-to-all-done.4 = bf16[16,16,128]{2,1,0:T(8,128)(2,1)S(1)} async-done(((bf16[16,16,128]{2,1,0:T(8,128)(2,1)}), bf16[16,16,128]{2,1,0:T(8,128)(2,1)S(1)}, u32[]{:S(2)}, u32[]{:S(2)}) %all-to-all-start.4) | async-done | bytes 65568 | tf_op jit(solution)/shard_map/all_to_all | solution.py:323
  124.4 10.1 %all-gather.2 = bf16[2048,128]{1,0:T(8,128)(2,1)S(1)} all-gather(bf16[512,128]{1,0:T(8,128)(2,1)S(1)} %pad_maximum_fusion), channel_id=4, replica_groups=mesh['z'=16,'y'=4,'x'=4,'c'=2] {'x'}, dimensions={0}, use_global_device_ids=true | all-gather | bytes 655360 | tf_op jit(solution)/shard_map/all_gather | solution.py:325
  134.5 8.8 %collective-permute-start.2 = (bf16[4,512,128]{2,1,0:T(8,128)(2,1)S(1)}, bf16[4,512,128]{2,1,0:T(8,128)(2,1)S(1)}, u32[]{:S(2)}, u32[]{:S(2)}) collective-permute-start(bf16[4,512,128]{2,1,0:T(8,128)(2,1)S(1)} %bitcast.15), channel_id=1, source_target_pairs={{0,1},{1,0},{2,3},{3,2},{4,5},{5,4},{6,7},{7,6},{8,9},{9,8},{10,11... | collective-permute-start | bytes 1572872 | tf_op jit(solution)/shard_map/ppermute | solution.py:264
  143.2 1.5 %collective-permute-done.2.other = bf16[4,512,128]{2,1,0:T(8,128)(2,1)S(1)} collective-permute-done((bf16[4,512,128]{2,1,0:T(8,128)(2,1)S(1)}, bf16[4,512,128]{2,1,0:T(8,128)(2,1)S(1)}, u32[]{:S(2)}, u32[]{:S(2)}) %collective-permute-start.2) | collective-permute-done | bytes 524320 | tf_op jit(solution)/shard_map/ppermute | solution.py:264
  144.8 0.0 copy-done
  144.8 0.0 copy-done.1
  144.8 1.4 shard_map.113
  (11 shorter events, 0.0 us)
Async XLA Ops:
  0.0 23.5 %copy-start.2 = (bf16[128,2048]{1,0:T(8,128)(2,1)S(1)}, bf16[128,2048]{1,0:T(8,128)(2,1)}, u32[]{:S(2)}) copy-start(bf16[128,2048]{1,0:T(8,128)(2,1)} %wq.1) | copy-start | bytes 1572868
  11.4 12.1 %copy-start.3 = (f32[2048]{0:T(1024)S(1)}, f32[2048]{0:T(1024)}, u32[]{:S(2)}) copy-start(f32[2048]{0:T(1024)} %param.12) | copy-start | bytes 24580
  11.4 12.1 %collective-permute-start = (bf16[4,256,256]{2,1,0:T(8,128)(2,1)S(1)}, bf16[4,256,256]{2,1,0:T(8,128)(2,1)S(1)}, u32[]{:S(2)}, u32[]{:S(2)}) collective-permute-start(bf16[4,256,256]{2,1,0:T(8,128)(2,1)S(1)} %bitcast.17), channel_id=1, source_target_pairs={{0,1},{1,0},{2,3},{3,2},{4,5},{5,4},{6,7},{7,6},{8,9},{9,8},{10,11... | collective-permute-start | bytes 1572872 | tf_op jit(solution)/shard_map/ppermute | solution.py:264
  23.5 0.7 copy-start.4
  23.5 0.7 copy-start.5
  23.5 0.7 copy-start.6
  61.6 24.4 %all-to-all-start.2 = ((bf16[8,16,32,128]{3,2,1,0:T(8,128)(2,1)}), bf16[8,16,32,128]{3,2,1,0:T(8,128)(2,1)S(1)}, u32[]{:S(2)}, u32[]{:S(2)}) async-start(bf16[8,16,32,128]{3,2,1,0:T(8,128)(2,1)} %broadcast_in_dim.2), calls=%async_computation.2 | async-start | bytes 2097152 | tf_op jit(solution)/shard_map/all_to_all | solution.py:260
  107.8 16.6 %all-to-all-start.4 = ((bf16[16,16,128]{2,1,0:T(8,128)(2,1)}), bf16[16,16,128]{2,1,0:T(8,128)(2,1)S(1)}, u32[]{:S(2)}, u32[]{:S(2)}) async-start(bf16[16,16,128]{2,1,0:T(8,128)(2,1)} %shard_map.111), calls=%async_computation.4 | async-start | bytes 131072 | tf_op jit(solution)/shard_map/all_to_all | solution.py:323
  112.8 2.9 %collective-permute-start.1 = (bf16[16,128]{1,0:T(8,128)(2,1)S(1)}, bf16[16,128]{1,0:T(8,128)(2,1)S(1)}, u32[]{:S(2)}, u32[]{:S(2)}) collective-permute-start(bf16[16,128]{1,0:T(8,128)(2,1)S(1)} %slice.15), channel_id=1, source_target_pairs={{0,8},{8,16},{16,24},{24,32},{32,40},{40,48},{48,56},{56,64},{64,7... | collective-permute-start | bytes 12296 | tf_op jit(solution)/shard_map/ppermute | solution.py:319
  115.1 29.7 %copy-start = (bf16[1024,256]{1,0:T(8,128)(2,1)S(1)}, bf16[1024,256]{1,0:T(8,128)(2,1)}, u32[]{:S(2)}) copy-start(bf16[1024,256]{1,0:T(8,128)(2,1)} %wpo.1) | copy-start | bytes 1572868
  115.1 29.7 %copy-start.1 = (bf16[1024,256]{1,0:T(8,128)(2,1)S(1)}, bf16[1024,256]{1,0:T(8,128)(2,1)}, u32[]{:S(2)}) copy-start(bf16[1024,256]{1,0:T(8,128)(2,1)} %wao.1) | copy-start | bytes 1572868
  134.5 10.3 %collective-permute-start.2 = (bf16[4,512,128]{2,1,0:T(8,128)(2,1)S(1)}, bf16[4,512,128]{2,1,0:T(8,128)(2,1)S(1)}, u32[]{:S(2)}, u32[]{:S(2)}) collective-permute-start(bf16[4,512,128]{2,1,0:T(8,128)(2,1)S(1)} %bitcast.15), channel_id=1, source_target_pairs={{0,1},{1,0},{2,3},{3,2},{4,5},{5,4},{6,7},{7,6},{8,9},{9,8},{10,11... | collective-permute-start | bytes 1572872 | tf_op jit(solution)/shard_map/ppermute | solution.py:264

commit v4 on v3

--- a/solution.py
+++ b/solution.py
@@ -49,7 +49,11 @@
 ):
     c = where[0]
     pairs = ((wk_, wk), (wv_, wv), (wp_, wp))
-    copies = [pltpu.make_async_copy(a, b, sems.at[k]) for k, (a, b) in enumerate(pairs)]
+    copies = []
+    for k, (a, b) in enumerate(pairs):
+        for j in range(4):
+            part = pl.ds(32 * j, 32)
+            copies.append(pltpu.make_async_copy(a.at[part], b.at[part], sems.at[4 * k + j]))
     for copy in copies:
         copy.start()
     total = jnp.zeros((ROWS, 1), F32)
@@ -65,10 +69,14 @@
             normed[:, pl.ds(at, 256)] = v.astype(BF16)
     rows = normed[...]
     q = head_scale(dot_t(rows, wq[...]), qg[...], HEAD ** (-0.5))
-    for copy in copies:
+    for copy in copies[0:4]:
         copy.wait()
     k = head_scale(dot_t(rows, wk[...]), kg[...], None)
+    for copy in copies[4:8]:
+        copy.wait()
     v = dot_t(rows, wv[...])
+    for copy in copies[8:12]:
+        copy.wait()
     pool[...] = dot_t(rows, wp[...]).astype(BF16)
     for h in range(2):
         kv = jnp.concatenate([k[h], v[:, h * HEAD : (h + 1) * HEAD]], axis=-1).astype(BF16)
@@ -86,92 +94,78 @@
             msg[s, h, 48:56, :] = lines
 
 
-def attend_kernel(where, ks, qy, gates, out, kv, vt, qs, gap, buf, lse):
+def place(i, t):
+    if t <= i:
+        return i, (i, *range(i))[t], 0
+    return 7 - i, t - i - 1, 1
+
+
+def prepare_kernel(where, qy, gates, qs, side, mask):
     y, s = where[0], where[1]
     lane = iota((16, 128), 1)
     for z in range(NZ):
-        for k in range(8):
-            kv[z * 256 + 32 * k : z * 256 + 32 * k + 32, 0:128] = ks[k, z]
-        g = gates[z].astype(F32).T
-        pad = jnp.zeros((128, 120), F32)
-        for j in range(2):
-            part = jnp.where(iota((128, 8), 1) // 4 == j, g, 0.0)
-            at = z * 256 + 128 * j
-            kv[at : at + 128, 128:256] = jnp.concatenate([part, pad], axis=1).astype(BF16)
-            vt[:, at : at + 128] = kv[at : at + 128, 0:128].T[64:128]
         for yy in range(NY):
             p = qy[yy, z].astype(F32)
             for half in range(2):
                 base = half * 128 + yy * 32 + (z % 2) * 16
                 q = p if half == 0 else pltpu.roll(p, 64, 1)
                 qs[z // 2, base : base + 16, 0:128] = jnp.where(lane < 64, q, 0.0).astype(BF16)
-    ln = iota((256, 128), 1)
-    signs = jnp.where((ln < 7) & (ln != 3), -1.0, 0.0).astype(BF16)
+    side[...] = gates[...].astype(F32).reshape(128, 128).T
     for m in range(8):
-        qs[m, :, 128:256] = signs
+        qs[m, :, 128:256] = jnp.full((256, 128), -1.0, BF16)
     r = iota((512, 256), 0)
     l = iota((512, 256), 1)
     k_at = ((r // 256) * 4 + y) * 256 + r % 256
     q_at = (((l // 16) % 2) * 4 + (l // 32) % 4) * 256 + 32 * s + (l // 128) * 16 + l % 16
-    gap[...] = k_at - q_at
-
-    def step(i, carry):
-        low = jnp.full((8, 256), NEG, F32)
-        tops = [low, low]
+    mask[...] = jnp.where(k_at <= q_at, 0.0, NEG)
+
+
+def attend_kernel(ks, qs, side, mask, out, kv, vt, buf_a, buf_b, lse):
+    for z in range(NZ):
+        for k in range(8):
+            kv[z * 256 + 32 * k : z * 256 + 32 * k + 32, 0:128] = ks[k, z]
+        for j in range(2):
+            at = z * 256 + 128 * j
+            mine = iota((128, 128), 1) // 4 == 2 * z + j
+            kv[at : at + 128, 128:256] = jnp.where(mine, side[...], 0.0).astype(BF16)
+            vt[:, at : at + 128] = kv[at : at + 128, 0:128].T[64:128]
+
+    def logits_of(i, buf):
+        tops = [None, None]
         for t in range(9):
-            first = t <= i
-            qi = jnp.where(first, i, 7 - i)
-            j = jnp.where(first, t, t - i - 1)
-            keys = kv[pl.ds(pl.multiple_of(j * 512, 512), 512), :]
-            logits = dot_t(keys, qs[qi])
-            logits = jnp.where(gap[...] <= 2048 * (qi - j), logits, NEG)
-            buf[t] = logits
-            m = jnp.max(logits.reshape(64, 8, 256), axis=0)
-            if t == 0:
-                tops[0] = m
-            elif t >= 4:
-                tops[1] = jnp.maximum(tops[1], m)
-            else:
-                tops[0] = jnp.where(first, jnp.maximum(tops[0], m), tops[0])
-                tops[1] = jnp.where(first, tops[1], jnp.maximum(tops[1], m))
-        tops = [jnp.maximum(jnp.max(m, axis=0, keepdims=True), -1e29) for m in tops]
-        sums = [jnp.zeros((8, 256), F32)] * 2
-        accs = [jnp.zeros((64, 256), F32)] * 2
+            qi, j, k = place(i, t)
+            v = dot_t(kv[512 * j : 512 * j + 512, :], qs[qi])
+            if qi == j:
+                v = v + mask[...]
+            buf[t] = v
+            m = jnp.max(v.reshape(64, 8, 256), axis=0)
+            tops[k] = m if tops[k] is None else jnp.maximum(tops[k], m)
+        return [jnp.maximum(jnp.max(m, axis=0, keepdims=True), -1e29) for m in tops]
+
+    def weigh(i, buf, tops):
+        sums, accs = [0.0, 0.0], [0.0, 0.0]
         for t in range(9):
-            first = t <= i
-            j = jnp.where(first, t, t - i - 1)
-            if t == 0:
-                m = tops[0]
-            elif t >= 4:
-                m = tops[1]
-            else:
-                m = jnp.where(first, tops[0], tops[1])
-            w = jnp.exp(buf[t] - m)
-            n = jnp.sum(w.reshape(64, 8, 256), axis=0)
-            a = dot(vt[:, pl.ds(pl.multiple_of(j * 512, 512), 512)], w.astype(BF16))
-            if t == 0:
-                sums[0], accs[0] = n, a
-            elif t >= 4:
-                sums[1], accs[1] = sums[1] + n, accs[1] + a
-            else:
-                sums[0] = jnp.where(first, sums[0] + n, sums[0])
-                accs[0] = jnp.where(first, accs[0] + a, accs[0])
-                sums[1] = jnp.where(first, sums[1], sums[1] + n)
-                accs[1] = jnp.where(first, accs[1], accs[1] + a)
-        for k in range(2):
+            _, j, k = place(i, t)
+            w = jnp.exp(buf[t] - tops[k])
+            sums[k] = sums[k] + jnp.sum(w.reshape(64, 8, 256), axis=0)
+            accs[k] = accs[k] + dot(vt[:, 512 * j : 512 * j + 512], w.astype(BF16))
+        for k, m in ((0, i), (1, 7 - i)):
             n = jnp.sum(sums[k], axis=0, keepdims=True)
             some = n > 0.0
             safe = jnp.where(some, n, 1.0)
-            m = i if k == 0 else 7 - i
-            lse[pl.ds(m, 1), :] = jnp.where(some, tops[k] + jnp.log(safe), NEG)
+            lse[m : m + 1, :] = jnp.where(some, tops[k] + jnp.log(safe), NEG)
             o = accs[k] / safe
             o = jnp.concatenate([o[:, 0:128], o[:, 128:256]], axis=0).T.astype(BF16)
             for yy in range(NY):
-                at = pl.multiple_of(m * 32, 32)
-                out[yy, pl.ds(at, 32), :] = o[32 * yy : 32 * yy + 32]
-        return carry
-
-    lax.fori_loop(0, 4, step, 0)
+                out[yy, 32 * m : 32 * m + 32, :] = o[32 * yy : 32 * yy + 32]
+
+    bufs = (buf_a, buf_b)
+    tops = logits_of(0, buf_a)
+    for i in range(4):
+        if i < 3:
+            later = logits_of(i + 1, bufs[(i + 1) % 2])
+        weigh(i, bufs[i % 2], tops)
+        tops = later
     ln = iota((8, 128), 1)
     for yy in range(NY):
         a = pltpu.roll(lse[:, 0:128], (128 - 32 * yy) % 128, 1)
@@ -180,7 +174,7 @@
         out[yy, 256:280, :] = jnp.concatenate(three_parts(v), axis=0).astype(BF16)
 
 
-def merge_kernel(where, parts, out):
+def merge_kernel(parts, out):
     lses = []
     for k in range(NY):
         v = parts[k, 256:280, :].astype(F32)
@@ -242,16 +236,17 @@
 
 
 def call(kernel, where, ins, outs, scratch, flops, mib, in_hbm=()):
-    shapes = [jax.ShapeDtypeStruct(s, BF16) for s in outs]
+    head = [jnp.stack([jnp.asarray(w, jnp.int32) for w in where])] if where else []
+    shapes = [jax.ShapeDtypeStruct(s, F32 if s in ((512, 256), (128, 128)) else BF16) for s in outs]
     return pl.pallas_call(
         kernel,
         out_shape=shapes,
-        in_specs=[SM] + [HB if k in in_hbm else VM for k in range(len(ins))],
+        in_specs=[SM] * len(head) + [HB if k in in_hbm else VM for k in range(len(ins))],
         out_specs=[VM] * len(outs),
         scratch_shapes=scratch,
         cost_estimate=pl.CostEstimate(flops=flops, bytes_accessed=2**20, transcendentals=0),
         compiler_params=pltpu.CompilerParams(vmem_limit_bytes=mib * 2**20),
-    )(jnp.stack([jnp.asarray(w, jnp.int32) for w in where]), *ins)
+    )(*head, *ins)
 
 
 def spread(value, axis):
@@ -288,7 +283,7 @@
         [(8, 2, 56, 128), (ROWS, 128)],
         [pltpu.VMEM((ROWS, 2048), BF16)]
         + [pltpu.VMEM((128, 2048), BF16)] * 3
-        + [pltpu.SemaphoreType.DMA((3,))],
+        + [pltpu.SemaphoreType.DMA((12,))],
         2 * ROWS * 2048 * 512,
         52,
         (4, 5, 6),
@@ -298,24 +293,32 @@
     mine = lax.all_to_all(heads.reshape(16, 56, 128), "z", 0, 0, tiled=True)
     ks = spread(mine[:, 0:32], TP)
     qy = lax.all_gather(mine[:, 32:48], "y", axis=0, tiled=False)
+    qs, side, mask = call(
+        prepare_kernel,
+        (y, 2 * x + c),
+        (qy, mine[:, 48:56]),
+        [(8, 256, 256), (128, 128), (512, 256)],
+        [],
+        2**20,
+        8,
+    )
     (parts,) = call(
         attend_kernel,
-        (y, 2 * x + c),
-        (ks, qy, mine[:, 48:56]),
+        (),
+        (ks, qs, side, mask),
         [(NY, 280, 128)],
         [
             pltpu.VMEM((4096, 256), BF16),
             pltpu.VMEM((64, 4096), BF16),
-            pltpu.VMEM((8, 256, 256), BF16),
-            pltpu.VMEM((512, 256), jnp.int32),
+            pltpu.VMEM((9, 512, 256), F32),
             pltpu.VMEM((9, 512, 256), F32),
             pltpu.VMEM((8, 256), F32),
         ],
         4 * 72 * 256 * 256 * 128,
-        24,
+        28,
     )
     parts = lax.all_to_all(parts, "y", 0, 0, tiled=True)
-    (merged,) = call(merge_kernel, (c,), (parts,), [(16, 16, 128)], [], 2**20, 8)
+    (merged,) = call(merge_kernel, (), (parts,), [(16, 16, 128)], [], 2**20, 8)
     rim = lax.ppermute(pool[ROWS - 16 :], SP, [(k, k + 1) for k in range(count - 1)])
     (pooled,) = call(
         pool_kernel, (x, (z * NY + y) * ROWS), (rim, pool), [(ROWS, 128)], [], 2**20, 4

time: 147 us -> 144 us (0.980)
  Pallas kernels: 17.7 us -> 15.4 us
    pallas_call x5 -> x6, Pallas kernels: 17.7 us -> 15.4 us  [call(): pl.pallas_call(kernel, out_shape=shapes, in_specs=[SM] * len(head) + [HB...]
  transfers between devices with their start and end apart: 5 -> 5, of which waited for: 5 -> 5; matrix products, arithmetic and copies ran while one was open for 0% -> 0% of each run, Pallas kernels for 0% -> 1%
where the time goes in v4:
time: 144 us; the launch traced here: 143 us
  blocking collectives  74.7 us (52%)
  starting transfers between devices  35.9 us (25%)
  Pallas kernels  15.4 us (11%)
  waiting for transfers between devices  14.8 us (10%)
  local copies, waits for them, and re-layouts  1.86 us (1%)
    all_to_all x1, blocking collectives, layer(): mine = lax.all_to_all(heads.reshape(16, 56, 128), 'z', 0, 0, tiled=True)  23.7 us
    ppermute x2, starting transfers between devices, swap(): return lax.ppermute(value, 'c', [(0, 1), (1, 0)])  19.3 us
    pallas_call x6, Pallas kernels, call(): pl.pallas_call(kernel, out_shape=shapes, in_specs=[SM] * len(head) + [HB...  15.4 us
    all_gather x1, blocking collectives, layer(): own = lax.all_gather(tokens, 'x', axis=0, tiled=False)  11.4 us
    all_gather x1, blocking collectives, layer(): qy = lax.all_gather(mine[:, 32:48], 'y', axis=0, tiled=False)  10.8 us
    all_gather x1, blocking collectives, layer(): own = lax.all_gather(both, 'x', axis=0, tiled=False)  10.1 us
    all_to_all x1, blocking collectives, layer(): parts = lax.all_to_all(parts, 'y', 0, 0, tiled=True)  9.65 us
    all_to_all x1, starting transfers between devices, spread(): return lax.all_to_all(copies, axis, 0, 0, tiled=True)  9.36 us
  transfers between devices with their start and end apart: 5, of which 5 were waited for; matrix products, arithmetic and copies ran while one was open for 0% of the time, Pallas kernels for 1%

profile of v4, /device:TPU:1, one launch (start us, length us, event | category | flops | bytes accessed | tf_op | source)
XLA Modules:
  0.0 143.0 jit_solution(4694851985895010379)
XLA Ops:
  0.0 11.4 %all-gather = bf16[1024,256]{1,0:T(8,128)(2,1)S(1)} all-gather(bf16[256,256]{1,0:T(8,128)(2,1)} %param.11), channel_id=2, replica_groups=mesh['z'=16,'y'=4,'x'=4,'c'=2] {'x'}, dimensions={0}, use_global_device_ids=true | all-gather | bytes 655360 | tf_op jit(solution)/shard_map/all_gather | solution.py:266
  11.4 10.6 %collective-permute-start = (bf16[4,256,256]{2,1,0:T(8,128)(2,1)S(1)}, bf16[4,256,256]{2,1,0:T(8,128)(2,1)S(1)}, u32[]{:S(2)}, u32[]{:S(2)}) collective-permute-start(bf16[4,256,256]{2,1,0:T(8,128)(2,1)S(1)} %bitcast.17), channel_id=1, source_target_pairs={{0,1},{1,0},{2,3},{3,2},{4,5},{5,4},{6,7},{7,6},{8,9},{9,8},{10,11... | collective-permute-start | bytes 1572872 | tf_op jit(solution)/shard_map/ppermute | solution.py:259
  22.0 1.5 %collective-permute-done.other = bf16[4,256,256]{2,1,0:T(8,128)(2,1)S(1)} collective-permute-done((bf16[4,256,256]{2,1,0:T(8,128)(2,1)S(1)}, bf16[4,256,256]{2,1,0:T(8,128)(2,1)S(1)}, u32[]{:S(2)}, u32[]{:S(2)}) %collective-permute-start) | collective-permute-done | bytes 524320 | tf_op jit(solution)/shard_map/ppermute | solution.py:259
  23.5 0.0 copy-done.2
  23.5 0.0 copy-done.3
  23.5 0.7 copy-done.4
  24.2 0.0 copy-done.5
  24.2 0.0 copy-done.6
  24.2 4.6 %shard_map.109 = (bf16[8,2,56,128]{3,2,1,0:T(8,128)(2,1)S(1)}, bf16[256,128]{1,0:T(8,128)(2,1)S(1)}) custom-call(s32[1]{0:T(128)} %bitcast.where, bf16[4,256,256]{2,1,0:T(8,128)(2,1)S(1)} %bitcast.18, bf16[4,256,256]{2,1,0:T(8,128)(2,1)S(1)} %collective-permute-done.other, f32[1,2048]{1,0:T(1,128)S(1)} %bitcast.21, bf16[128,2048]{1,0:T(8,128)(2,1)S(1)} %copy-done.2, ...), custom_call_target="tpu_custom_call" | custom-call | flops 536870912 | bytes 1048576 | tf_op jit(solution)/shard_map/pallas_call | solution.py:241
  28.8 9.1 %all_to_all.25 = bf16[8,112,128]{2,1,0:T(8,128)(2,1)S(1)} all-to-all(bf16[8,112,128]{2,1,0:T(8,128)(2,1)S(1)} %bitcast.20), channel_id=1, replica_groups=mesh['z'=16,'y'=4,'x'=4,'c'=2] {'x','c'}, dimensions={0} | all-to-all | bytes 458752 | tf_op jit(solution)/shard_map/all_to_all | solution.py:292
  37.9 23.7 %all_to_all.26 = bf16[16,56,128]{2,1,0:T(8,128)(2,1)S(1)} all-to-all(bf16[16,56,128]{2,1,0:T(8,128)(2,1)S(1)} %bitcast.25), channel_id=1, replica_groups=mesh['z'=16,'y'=4,'x'=4,'c'=2] {'z'}, dimensions={0} | all-to-all | bytes 458752 | tf_op jit(solution)/shard_map/all_to_all | solution.py:293
  61.6 1.2 broadcast_in_dim.2
  62.8 9.4 %all-to-all-start.2 = ((bf16[8,16,32,128]{3,2,1,0:T(8,128)(2,1)}), bf16[8,16,32,128]{3,2,1,0:T(8,128)(2,1)S(1)}, u32[]{:S(2)}, u32[]{:S(2)}) async-start(bf16[8,16,32,128]{3,2,1,0:T(8,128)(2,1)} %broadcast_in_dim.2), calls=%async_computation.2 | async-start | bytes 2097152 | tf_op jit(solution)/shard_map/all_to_all | solution.py:255
  72.1 0.1 pad_add_fusion.where
  72.2 10.8 %all-gather.1 = bf16[64,16,128]{2,1,0:T(8,128)(2,1)S(1)} all-gather(bf16[16,16,128]{2,1,0:T(8,128)(2,1)S(1)} %slice.17), channel_id=3, replica_groups=mesh['z'=16,'y'=4,'x'=4,'c'=2] {'y'}, dimensions={0}, use_global_device_ids=true | all-gather | bytes 327680 | tf_op jit(solution)/shard_map/all_gather | solution.py:295
  83.0 0.9 shard_map.110
  83.9 3.3 %all-to-all-done.2.ks = bf16[8,16,32,128]{3,2,1,0:T(8,128)(2,1)S(1)} async-done(((bf16[8,16,32,128]{3,2,1,0:T(8,128)(2,1)}), bf16[8,16,32,128]{3,2,1,0:T(8,128)(2,1)S(1)}, u32[]{:S(2)}, u32[]{:S(2)}) %all-to-all-start.2) | async-done | bytes 1048608 | tf_op jit(solution)/shard_map/all_to_all | solution.py:255
  87.1 6.8 %shard_map.111 = bf16[4,280,128]{2,1,0:T(8,128)(2,1)S(1)} custom-call(bf16[8,16,32,128]{3,2,1,0:T(8,128)(2,1)S(1)} %all-to-all-done.2.ks, bf16[8,256,256]{2,1,0:T(8,128)(2,1)S(1)} %get-tuple-element.11.qs, f32[128,128]{1,0:T(8,128)S(1)} %get-tuple-element.12.side, f32[512,256]{1,0:T(8,128)S(1)} %get-tuple-element.13.mask), custom_call_target="tpu_custom_call" | custom-call | flops 2415919104 | bytes 1048576 | tf_op jit(solution)/shard_map/pallas_call | solution.py:241
  93.9 9.6 %all_to_all.27.parts = bf16[4,280,128]{2,1,0:T(8,128)(2,1)S(1)} all-to-all(bf16[4,280,128]{2,1,0:T(8,128)(2,1)S(1)} %shard_map.111), channel_id=1, replica_groups=mesh['z'=16,'y'=4,'x'=4,'c'=2] {'y'}, dimensions={0} | all-to-all | bytes 573440 | tf_op jit(solution)/shard_map/all_to_all | solution.py:320
  103.5 1.1 shard_map.112
  104.6 5.0 %all-to-all-start.4 = ((bf16[16,16,128]{2,1,0:T(8,128)(2,1)}), bf16[16,16,128]{2,1,0:T(8,128)(2,1)S(1)}, u32[]{:S(2)}, u32[]{:S(2)}) async-start(bf16[16,16,128]{2,1,0:T(8,128)(2,1)} %shard_map.112), calls=%async_computation.4 | async-start | bytes 131072 | tf_op jit(solution)/shard_map/all_to_all | solution.py:326
  109.7 2.2 %collective-permute-start.1 = (bf16[16,128]{1,0:T(8,128)(2,1)S(1)}, bf16[16,128]{1,0:T(8,128)(2,1)S(1)}, u32[]{:S(2)}, u32[]{:S(2)}) collective-permute-start(bf16[16,128]{1,0:T(8,128)(2,1)S(1)} %slice.15), channel_id=1, source_target_pairs={{0,8},{8,16},{16,24},{24,32},{32,40},{40,48},{48,56},{56,64},{64,7... | collective-permute-start | bytes 12296 | tf_op jit(solution)/shard_map/ppermute | solution.py:322
  111.9 0.1 pad_add_fusion.1.where
  111.9 0.7 collective-permute-done.1.rim
  112.6 0.7 shard_map.113
  113.3 7.9 %all-to-all-done.4 = bf16[16,16,128]{2,1,0:T(8,128)(2,1)S(1)} async-done(((bf16[16,16,128]{2,1,0:T(8,128)(2,1)}), bf16[16,16,128]{2,1,0:T(8,128)(2,1)S(1)}, u32[]{:S(2)}, u32[]{:S(2)}) %all-to-all-start.4) | async-done | bytes 65568 | tf_op jit(solution)/shard_map/all_to_all | solution.py:326
  121.2 10.1 %all-gather.2 = bf16[2048,128]{1,0:T(8,128)(2,1)S(1)} all-gather(bf16[512,128]{1,0:T(8,128)(2,1)S(1)} %pad_maximum_fusion), channel_id=4, replica_groups=mesh['z'=16,'y'=4,'x'=4,'c'=2] {'x'}, dimensions={0}, use_global_device_ids=true | all-gather | bytes 655360 | tf_op jit(solution)/shard_map/all_gather | solution.py:328
  131.3 8.8 %collective-permute-start.2 = (bf16[4,512,128]{2,1,0:T(8,128)(2,1)S(1)}, bf16[4,512,128]{2,1,0:T(8,128)(2,1)S(1)}, u32[]{:S(2)}, u32[]{:S(2)}) collective-permute-start(bf16[4,512,128]{2,1,0:T(8,128)(2,1)S(1)} %bitcast.15), channel_id=1, source_target_pairs={{0,1},{1,0},{2,3},{3,2},{4,5},{5,4},{6,7},{7,6},{8,9},{9,8},{10,11... | collective-permute-start | bytes 1572872 | tf_op jit(solution)/shard_map/ppermute | solution.py:259
  140.1 1.5 %collective-permute-done.2.other = bf16[4,512,128]{2,1,0:T(8,128)(2,1)S(1)} collective-permute-done((bf16[4,512,128]{2,1,0:T(8,128)(2,1)S(1)}, bf16[4,512,128]{2,1,0:T(8,128)(2,1)S(1)}, u32[]{:S(2)}, u32[]{:S(2)}) %collective-permute-start.2) | collective-permute-done | bytes 524320 | tf_op jit(solution)/shard_map/ppermute | solution.py:259
  141.6 0.0 copy-done
  141.6 0.0 copy-done.1
  141.6 1.4 shard_map.114
  (12 shorter events, 0.0 us)
Async XLA Ops:
  0.0 23.5 %copy-start.2 = (bf16[128,2048]{1,0:T(8,128)(2,1)S(1)}, bf16[128,2048]{1,0:T(8,128)(2,1)}, u32[]{:S(2)}) copy-start(bf16[128,2048]{1,0:T(8,128)(2,1)} %wq.1) | copy-start | bytes 1572868
  11.4 12.1 %copy-start.3 = (f32[2048]{0:T(1024)S(1)}, f32[2048]{0:T(1024)}, u32[]{:S(2)}) copy-start(f32[2048]{0:T(1024)} %param.12) | copy-start | bytes 24580
  11.4 12.1 %collective-permute-start = (bf16[4,256,256]{2,1,0:T(8,128)(2,1)S(1)}, bf16[4,256,256]{2,1,0:T(8,128)(2,1)S(1)}, u32[]{:S(2)}, u32[]{:S(2)}) collective-permute-start(bf16[4,256,256]{2,1,0:T(8,128)(2,1)S(1)} %bitcast.17), channel_id=1, source_target_pairs={{0,1},{1,0},{2,3},{3,2},{4,5},{5,4},{6,7},{7,6},{8,9},{9,8},{10,11... | collective-permute-start | bytes 1572872 | tf_op jit(solution)/shard_map/ppermute | solution.py:259
  23.5 0.7 copy-start.4
  23.5 0.7 copy-start.5
  23.5 0.7 copy-start.6
  62.8 24.4 %all-to-all-start.2 = ((bf16[8,16,32,128]{3,2,1,0:T(8,128)(2,1)}), bf16[8,16,32,128]{3,2,1,0:T(8,128)(2,1)S(1)}, u32[]{:S(2)}, u32[]{:S(2)}) async-start(bf16[8,16,32,128]{3,2,1,0:T(8,128)(2,1)} %broadcast_in_dim.2), calls=%async_computation.2 | async-start | bytes 2097152 | tf_op jit(solution)/shard_map/all_to_all | solution.py:255
  104.6 16.6 %all-to-all-start.4 = ((bf16[16,16,128]{2,1,0:T(8,128)(2,1)}), bf16[16,16,128]{2,1,0:T(8,128)(2,1)S(1)}, u32[]{:S(2)}, u32[]{:S(2)}) async-start(bf16[16,16,128]{2,1,0:T(8,128)(2,1)} %shard_map.112), calls=%async_computation.4 | async-start | bytes 131072 | tf_op jit(solution)/shard_map/all_to_all | solution.py:326
  109.7 2.9 %collective-permute-start.1 = (bf16[16,128]{1,0:T(8,128)(2,1)S(1)}, bf16[16,128]{1,0:T(8,128)(2,1)S(1)}, u32[]{:S(2)}, u32[]{:S(2)}) collective-permute-start(bf16[16,128]{1,0:T(8,128)(2,1)S(1)} %slice.15), channel_id=1, source_target_pairs={{0,8},{8,16},{16,24},{24,32},{32,40},{40,48},{48,56},{56,64},{64,7... | collective-permute-start | bytes 12296 | tf_op jit(solution)/shard_map/ppermute | solution.py:322
  111.9 29.7 %copy-start = (bf16[1024,256]{1,0:T(8,128)(2,1)S(1)}, bf16[1024,256]{1,0:T(8,128)(2,1)}, u32[]{:S(2)}) copy-start(bf16[1024,256]{1,0:T(8,128)(2,1)} %wpo.1) | copy-start | bytes 1572868
  111.9 29.7 %copy-start.1 = (bf16[1024,256]{1,0:T(8,128)(2,1)S(1)}, bf16[1024,256]{1,0:T(8,128)(2,1)}, u32[]{:S(2)}) copy-start(bf16[1024,256]{1,0:T(8,128)(2,1)} %wao.1) | copy-start | bytes 1572868
  131.3 10.3 %collective-permute-start.2 = (bf16[4,512,128]{2,1,0:T(8,128)(2,1)S(1)}, bf16[4,512,128]{2,1,0:T(8,128)(2,1)S(1)}, u32[]{:S(2)}, u32[]{:S(2)}) collective-permute-start(bf16[4,512,128]{2,1,0:T(8,128)(2,1)S(1)} %bitcast.15), channel_id=1, source_target_pairs={{0,1},{1,0},{2,3},{3,2},{4,5},{5,4},{6,7},{7,6},{8,9},{9,8},{10,11... | collective-permute-start | bytes 1572872 | tf_op jit(solution)/shard_map/ppermute | solution.py:259

commit v5 on v4

--- a/solution.py
+++ b/solution.py
@@ -12,6 +12,7 @@
 EPS = 1e-06
 NEG = -1e30
 ROWS = 256
+SUB = 32
 NZ, NY, NX, NC = 16, 4, 4, 2
 TP = ("x", "c")
 SP = ("z", "y")
@@ -44,24 +45,27 @@
     return parts
 
 
+def early_kernel(own, squares):
+    total = jnp.zeros((ROWS, 128), F32)
+    for x in range(NX):
+        v = own[x].astype(F32)
+        total = total + v[:, 0:128] * v[:, 0:128] + v[:, 128:256] * v[:, 128:256]
+    squares[...] = total
+
+
 def project_kernel(
-    where, own, other, gain, wq, wk_, wv_, wp_, qg, kg, gate, msg, pool, normed, wk, wv, wp, sems
+    where, own, other, squares, gain, wq, wk, wv_, wp_, qg, kg, gate, msg, pool, normed, wv, wp, sems
 ):
     c = where[0]
-    pairs = ((wk_, wk), (wv_, wv), (wp_, wp))
     copies = []
-    for k, (a, b) in enumerate(pairs):
-        for j in range(4):
-            part = pl.ds(32 * j, 32)
-            copies.append(pltpu.make_async_copy(a.at[part], b.at[part], sems.at[4 * k + j]))
-    for copy in copies:
-        copy.start()
-    total = jnp.zeros((ROWS, 1), F32)
-    for x in range(NX):
-        for ref in (own, other):
-            v = ref[x].astype(F32)
-            total = total + jnp.sum(v * v, axis=-1, keepdims=True)
-    scale = lax.rsqrt(total / 2048.0 + EPS)
+    for k, (a, b) in enumerate(((wv_, wv), (wp_, wp))):
+        copies.append(pltpu.make_async_copy(a, b, sems.at[k]))
+        copies[k].start(priority=k)
+    total = squares[...]
+    for x in range(NX):
+        v = other[x].astype(F32)
+        total = total + v[:, 0:128] * v[:, 0:128] + v[:, 128:256] * v[:, 128:256]
+    scale = lax.rsqrt(jnp.sum(total, axis=-1, keepdims=True) / 2048.0 + EPS)
     for x in range(NX):
         for k, ref in enumerate((own, other)):
             at = pl.multiple_of((2 * x + (c if k == 0 else 1 - c)) * 256, 256)
@@ -69,15 +73,9 @@
             normed[:, pl.ds(at, 256)] = v.astype(BF16)
     rows = normed[...]
     q = head_scale(dot_t(rows, wq[...]), qg[...], HEAD ** (-0.5))
-    for copy in copies[0:4]:
-        copy.wait()
     k = head_scale(dot_t(rows, wk[...]), kg[...], None)
-    for copy in copies[4:8]:
-        copy.wait()
+    copies[0].wait()
     v = dot_t(rows, wv[...])
-    for copy in copies[8:12]:
-        copy.wait()
-    pool[...] = dot_t(rows, wp[...]).astype(BF16)
     for h in range(2):
         kv = jnp.concatenate([k[h], v[:, h * HEAD : (h + 1) * HEAD]], axis=-1).astype(BF16)
         g = three_parts(gate[h : h + 1, :])
@@ -92,6 +90,8 @@
             b = q[h][32 * s + 16 : 32 * s + 32]
             msg[s, h, 32:48, :] = jnp.concatenate([a, b], axis=-1).astype(BF16)
             msg[s, h, 48:56, :] = lines
+    copies[1].wait()
+    pool[...] = dot_t(rows, wp[...]).astype(BF16)
 
 
 def place(i, t):
@@ -210,22 +210,32 @@
     pooled[...] = (mean - now).astype(BF16)
 
 
-def output_kernel(where, own, other, wpo, wao, out, pooled, attended):
-    c = where[0]
+def half_output(s_of, ref, wpo, wao, attended, total, start):
     half = iota((16, 128), 1) < 64
     for x in range(NX):
-        for k, ref in enumerate((own, other)):
-            s = 2 * x + (c if k == 0 else 1 - c)
-            pooled[:, pl.ds(pl.multiple_of(s * 128, 128), 128)] = ref[x, 256:512, :]
-            for j in range(8):
-                a = ref[x, 32 * j : 32 * j + 16, :].astype(F32)
-                b = ref[x, 32 * j + 16 : 32 * j + 32, :].astype(F32)
-                u = jnp.where(half, a, pltpu.roll(b, 64, 1)).astype(BF16)
-                v = jnp.where(half, pltpu.roll(a, 64, 1), b).astype(BF16)
-                at = pl.multiple_of(s * 32, 32)
-                attended[pl.ds(at, 16), 128 * j : 128 * j + 128] = u
-                attended[pl.ds(at + 16, 16), 128 * j : 128 * j + 128] = v
-    out[...] = (dot(pooled[...], wpo[...]) + dot(attended[...], wao[...])).astype(BF16)
+        rows = wpo[pl.ds(pl.multiple_of(s_of(x) * 128, 128), 128), :]
+        start = start + dot(ref[x, 256:512, :], rows)
+        for j in range(8):
+            a = ref[x, 32 * j : 32 * j + 16, :].astype(F32)
+            b = ref[x, 32 * j + 16 : 32 * j + 32, :].astype(F32)
+            u = jnp.where(half, a, pltpu.roll(b, 64, 1)).astype(BF16)
+            v = jnp.where(half, pltpu.roll(a, 64, 1), b).astype(BF16)
+            attended[32 * x : 32 * x + 16, 128 * j : 128 * j + 128] = u
+            attended[32 * x + 16 : 32 * x + 32, 128 * j : 128 * j + 128] = v
+    total[...] = start
+    mine = dot(attended[...], wao[...])
+    for x in range(NX):
+        at = pl.ds(pl.multiple_of(s_of(x) * SUB, SUB), SUB)
+        total[at, :] = total[at, :] + mine[32 * x : 32 * x + 32]
+
+
+def first_kernel(where, own, wpo, wao, total, attended):
+    half_output(lambda x: 2 * x + where[0], own, wpo, wao, attended, total, 0.0)
+
+
+def last_kernel(where, other, first, wpo, wao, out, attended, total):
+    half_output(lambda x: 2 * x + 1 - where[0], other, wpo, wao, attended, total, first[...])
+    out[...] = total[...].astype(BF16)
 
 
 VM = pl.BlockSpec(memory_space=pltpu.VMEM)
@@ -237,7 +247,10 @@
 
 def call(kernel, where, ins, outs, scratch, flops, mib, in_hbm=()):
     head = [jnp.stack([jnp.asarray(w, jnp.int32) for w in where])] if where else []
-    shapes = [jax.ShapeDtypeStruct(s, F32 if s in ((512, 256), (128, 128)) else BF16) for s in outs]
+    shapes = []
+    for s in outs:
+        wide = s[-1] == F32
+        shapes.append(jax.ShapeDtypeStruct(s[:-1] if wide else s, F32 if wide else BF16))
     return pl.pallas_call(
         kernel,
         out_shape=shapes,
@@ -245,7 +258,7 @@
         out_specs=[VM] * len(outs),
         scratch_shapes=scratch,
         cost_estimate=pl.CostEstimate(flops=flops, bytes_accessed=2**20, transcendentals=0),
-        compiler_params=pltpu.CompilerParams(vmem_limit_bytes=mib * 2**20),
+        compiler_params=pltpu.CompilerParams(vmem_limit_bytes=int(mib * 2**20)),
     )(*head, *ins)
 
 
@@ -263,14 +276,16 @@
     tokens, norm_gain, wq, wk, wv, wp, query_gain, key_gain, cum_gate, wpo, wao
 ):
     z, y, x, c = (lax.axis_index(a) for a in ("z", "y", "x", "c"))
-    own = lax.all_gather(tokens, "x", axis=0, tiled=False)
+    own = spread(tokens, "x")
     other = swap(own)
+    (squares,) = call(early_kernel, (), (own,), [(ROWS, 128, F32)], [], 2**20, 4)
     msg, pool = call(
         project_kernel,
         (c,),
         (
             own,
             other,
+            squares,
             norm_gain.reshape(1, 2048),
             wq,
             wk,
@@ -282,11 +297,11 @@
         ),
         [(8, 2, 56, 128), (ROWS, 128)],
         [pltpu.VMEM((ROWS, 2048), BF16)]
-        + [pltpu.VMEM((128, 2048), BF16)] * 3
-        + [pltpu.SemaphoreType.DMA((12,))],
+        + [pltpu.VMEM((128, 2048), BF16)] * 2
+        + [pltpu.SemaphoreType.DMA((2,))],
         2 * ROWS * 2048 * 512,
-        52,
-        (4, 5, 6),
+        51.375,
+        (6, 7),
     )
     count = NZ * NY
     heads = lax.all_to_all(msg.reshape(8, 112, 128), TP, 0, 0, tiled=True)
@@ -297,7 +312,7 @@
         prepare_kernel,
         (y, 2 * x + c),
         (qy, mine[:, 48:56]),
-        [(8, 256, 256), (128, 128), (512, 256)],
+        [(8, 256, 256), (128, 128, F32), (512, 256, F32)],
         [],
         2**20,
         8,
@@ -325,16 +340,25 @@
     )
     back = lax.all_to_all(merged, "z", 0, 0, tiled=True)
     both = jnp.concatenate([back.reshape(256, 128), pooled], axis=0)
-    own = lax.all_gather(both, "x", axis=0, tiled=False)
+    own = spread(both, "x")
     other = swap(own)
+    (first,) = call(
+        first_kernel,
+        (c,),
+        (own, wpo, wao),
+        [(ROWS, 256, F32)],
+        [pltpu.VMEM((128, 1024), BF16)],
+        ROWS * 2048 * 256,
+        8,
+    )
     (mixed,) = call(
-        output_kernel,
+        last_kernel,
         (c,),
-        (own, other, wpo, wao),
+        (other, first, wpo, wao),
         [(ROWS, 256)],
-        [pltpu.VMEM((ROWS, 1024), BF16), pltpu.VMEM((ROWS, 1024), BF16)],
-        2 * ROWS * 2048 * 256,
-        12,
+        [pltpu.VMEM((128, 1024), BF16), pltpu.VMEM((ROWS, 256), F32)],
+        ROWS * 2048 * 256,
+        8,
     )
     return mixed
 

time: 144 us -> 140 us (0.972)
  starting transfers between devices: 35.9 us -> 31.4 us
    all_gather x2 -> x0, blocking collectives: 21.5 us -> none  [the longest x1 11.4 us: layer(): own = lax.all_gather(tokens, 'x', axis=0, tiled=False)]
    all_to_all x0 -> x2, blocking collectives: none -> 21.2 us  [spread(): return lax.all_to_all(copies, axis, 0, 0, tiled=True)]
    ppermute x2, starting transfers between devices: 19.3 us -> 14.8 us  [swap(): return lax.ppermute(value, 'c', [(0, 1), (1, 0)])]
    pallas_call x6 -> x8, Pallas kernels: 15.4 us -> 14.6 us  [call(): pl.pallas_call(kernel, out_shape=shapes, in_specs=[SM] * len(head) + [HB...]
where the time goes in v5:
time: 140 us; the launch traced here: 139 us
  blocking collectives  75.5 us (54%)
  starting transfers between devices  31.4 us (22%)
  Pallas kernels  14.6 us (10%)
  waiting for transfers between devices  14.3 us (10%)
  local copies, waits for them, and re-layouts  2.86 us (2%)
    all_to_all x1, blocking collectives, layer(): mine = lax.all_to_all(heads.reshape(16, 56, 128), 'z', 0, 0, tiled=True)  25 us
    all_to_all x2, blocking collectives, spread(): return lax.all_to_all(copies, axis, 0, 0, tiled=True)  21.2 us
    ppermute x2, starting transfers between devices, swap(): return lax.ppermute(value, 'c', [(0, 1), (1, 0)])  14.8 us
    pallas_call x8, Pallas kernels, call(): pl.pallas_call(kernel, out_shape=shapes, in_specs=[SM] * len(head) + [HB...  14.6 us
    all_gather x1, blocking collectives, layer(): qy = lax.all_gather(mine[:, 32:48], 'y', axis=0, tiled=False)  10.8 us
    all_to_all x1, blocking collectives, layer(): parts = lax.all_to_all(parts, 'y', 0, 0, tiled=True)  9.64 us
    all_to_all x1, starting transfers between devices, spread(): return lax.all_to_all(copies, axis, 0, 0, tiled=True)  9.36 us
    all_to_all x1, blocking collectives, layer(): heads = lax.all_to_all(msg.reshape(8, 112, 128), TP, 0, 0, tiled=True)  8.93 us
  transfers between devices with their start and end apart: 5, of which 5 were waited for; matrix products, arithmetic and copies ran while one was open for 0% of the time, Pallas kernels for 1%

profile of v5, /device:TPU:1, one launch (start us, length us, event | category | flops | bytes accessed | tf_op | source)
XLA Modules:
  0.0 139.0 jit_solution(5433557322561719507)
XLA Ops:
  0.0 0.9 broadcast_in_dim.6
  1.0 11.7 %all_to_all.35.own = bf16[4,256,256]{2,1,0:T(8,128)(2,1)S(1)} all-to-all(bf16[4,256,256]{2,1,0:T(8,128)(2,1)S(1)} %broadcast_in_dim.6), channel_id=1, replica_groups=mesh['z'=16,'y'=4,'x'=4,'c'=2] {'x'}, dimensions={0} | all-to-all | bytes 1048576 | tf_op jit(solution)/shard_map/all_to_all | solution.py:268
  12.7 7.8 %collective-permute-start = (bf16[4,256,256]{2,1,0:T(8,128)(2,1)S(1)}, bf16[4,256,256]{2,1,0:T(8,128)(2,1)S(1)}, u32[]{:S(2)}, u32[]{:S(2)}) collective-permute-start(bf16[4,256,256]{2,1,0:T(8,128)(2,1)S(1)} %all_to_all.35.own), channel_id=1, source_target_pairs={{0,1},{1,0},{2,3},{3,2},{4,5},{5,4},{6,7},{7,6},{8,9},{9,8},{10,11... | collective-permute-start | bytes 1572872 | tf_op jit(solution)/shard_map/ppermute | solution.py:272
  20.4 0.0 copy-start.5
  20.5 0.1 shard_map.109.squares
  20.6 1.4 collective-permute-done.other
  22.0 0.6 copy-done.6
  22.6 0.0 copy-done.7
  22.6 3.5 %shard_map.110 = (bf16[8,2,56,128]{3,2,1,0:T(8,128)(2,1)S(1)}, bf16[256,128]{1,0:T(8,128)(2,1)S(1)}) custom-call(s32[1]{0:T(128)} %bitcast.where, bf16[4,256,256]{2,1,0:T(8,128)(2,1)S(1)} %all_to_all.35.own, bf16[4,256,256]{2,1,0:T(8,128)(2,1)S(1)} %collective-permute-done.other, f32[256,128]{1,0:T(8,128)S(1)} %shard_map.109.squares, ...), custom_call_target="tpu_custom_call" | custom-call | flops 536870912 | bytes 1048576 | tf_op jit(solution)/shard_map/pallas_call | solution.py:254
  26.1 8.9 %all_to_all.36 = bf16[8,112,128]{2,1,0:T(8,128)(2,1)S(1)} all-to-all(bf16[8,112,128]{2,1,0:T(8,128)(2,1)S(1)} %bitcast.14), channel_id=1, replica_groups=mesh['z'=16,'y'=4,'x'=4,'c'=2] {'x','c'}, dimensions={0} | all-to-all | bytes 458752 | tf_op jit(solution)/shard_map/all_to_all | solution.py:307
  35.1 25.0 %all_to_all.37 = bf16[16,56,128]{2,1,0:T(8,128)(2,1)S(1)} all-to-all(bf16[16,56,128]{2,1,0:T(8,128)(2,1)S(1)} %bitcast.19), channel_id=1, replica_groups=mesh['z'=16,'y'=4,'x'=4,'c'=2] {'z'}, dimensions={0} | all-to-all | bytes 458752 | tf_op jit(solution)/shard_map/all_to_all | solution.py:308
  60.0 1.2 broadcast_in_dim.7
  61.2 9.4 %all-to-all-start.3 = ((bf16[8,16,32,128]{3,2,1,0:T(8,128)(2,1)}), bf16[8,16,32,128]{3,2,1,0:T(8,128)(2,1)S(1)}, u32[]{:S(2)}, u32[]{:S(2)}) async-start(bf16[8,16,32,128]{3,2,1,0:T(8,128)(2,1)} %broadcast_in_dim.7), calls=%async_computation.3 | async-start | bytes 2097152 | tf_op jit(solution)/shard_map/all_to_all | solution.py:268
  70.6 0.1 pad_add_fusion.where
  70.6 10.8 %all-gather = bf16[64,16,128]{2,1,0:T(8,128)(2,1)S(1)} all-gather(bf16[16,16,128]{2,1,0:T(8,128)(2,1)S(1)} %slice.17), channel_id=2, replica_groups=mesh['z'=16,'y'=4,'x'=4,'c'=2] {'y'}, dimensions={0}, use_global_device_ids=true | all-gather | bytes 327680 | tf_op jit(solution)/shard_map/all_gather | solution.py:310
  81.4 0.9 shard_map.111
  82.3 3.3 %all-to-all-done.3.ks = bf16[8,16,32,128]{3,2,1,0:T(8,128)(2,1)S(1)} async-done(((bf16[8,16,32,128]{3,2,1,0:T(8,128)(2,1)}), bf16[8,16,32,128]{3,2,1,0:T(8,128)(2,1)S(1)}, u32[]{:S(2)}, u32[]{:S(2)}) %all-to-all-start.3) | async-done | bytes 1048608 | tf_op jit(solution)/shard_map/all_to_all | solution.py:268
  85.6 6.9 %shard_map.112 = bf16[4,280,128]{2,1,0:T(8,128)(2,1)S(1)} custom-call(bf16[8,16,32,128]{3,2,1,0:T(8,128)(2,1)S(1)} %all-to-all-done.3.ks, bf16[8,256,256]{2,1,0:T(8,128)(2,1)S(1)} %get-tuple-element.11.qs, f32[128,128]{1,0:T(8,128)S(1)} %get-tuple-element.12.side, f32[512,256]{1,0:T(8,128)S(1)} %get-tuple-element.13.mask), custom_call_target="tpu_custom_call" | custom-call | flops 2415919104 | bytes 1048576 | tf_op jit(solution)/shard_map/pallas_call | solution.py:254
  92.5 9.6 %all_to_all.38.parts = bf16[4,280,128]{2,1,0:T(8,128)(2,1)S(1)} all-to-all(bf16[4,280,128]{2,1,0:T(8,128)(2,1)S(1)} %shard_map.112), channel_id=1, replica_groups=mesh['z'=16,'y'=4,'x'=4,'c'=2] {'y'}, dimensions={0} | all-to-all | bytes 573440 | tf_op jit(solution)/shard_map/all_to_all | solution.py:335
  102.1 1.1 shard_map.113
  103.2 5.0 %all-to-all-start.5 = ((bf16[16,16,128]{2,1,0:T(8,128)(2,1)}), bf16[16,16,128]{2,1,0:T(8,128)(2,1)S(1)}, u32[]{:S(2)}, u32[]{:S(2)}) async-start(bf16[16,16,128]{2,1,0:T(8,128)(2,1)} %shard_map.113), calls=%async_computation.5 | async-start | bytes 131072 | tf_op jit(solution)/shard_map/all_to_all | solution.py:341
  108.2 2.2 %collective-permute-start.1 = (bf16[16,128]{1,0:T(8,128)(2,1)S(1)}, bf16[16,128]{1,0:T(8,128)(2,1)S(1)}, u32[]{:S(2)}, u32[]{:S(2)}) collective-permute-start(bf16[16,128]{1,0:T(8,128)(2,1)S(1)} %slice.15), channel_id=1, source_target_pairs={{0,8},{8,16},{16,24},{24,32},{32,40},{40,48},{48,56},{56,64},{64,7... | collective-permute-start | bytes 12296 | tf_op jit(solution)/shard_map/ppermute | solution.py:337
  110.4 0.1 pad_add_fusion.1.where
  110.5 0.7 collective-permute-done.1.rim
  111.2 0.7 shard_map.114
  111.9 7.9 %all-to-all-done.5 = bf16[16,16,128]{2,1,0:T(8,128)(2,1)S(1)} async-done(((bf16[16,16,128]{2,1,0:T(8,128)(2,1)}), bf16[16,16,128]{2,1,0:T(8,128)(2,1)S(1)}, u32[]{:S(2)}, u32[]{:S(2)}) %all-to-all-start.5) | async-done | bytes 65568 | tf_op jit(solution)/shard_map/all_to_all | solution.py:341
  119.8 0.1 broadcast_in_dim.8
  119.9 9.5 %all_to_all.39.own = bf16[4,512,128]{2,1,0:T(8,128)(2,1)S(1)} all-to-all(bf16[4,512,128]{2,1,0:T(8,128)(2,1)S(1)} %broadcast_in_dim.8), channel_id=1, replica_groups=mesh['z'=16,'y'=4,'x'=4,'c'=2] {'x'}, dimensions={0} | all-to-all | bytes 1048576 | tf_op jit(solution)/shard_map/all_to_all | solution.py:268
  129.4 7.0 %collective-permute-start.2 = (bf16[4,512,128]{2,1,0:T(8,128)(2,1)S(1)}, bf16[4,512,128]{2,1,0:T(8,128)(2,1)S(1)}, u32[]{:S(2)}, u32[]{:S(2)}) collective-permute-start(bf16[4,512,128]{2,1,0:T(8,128)(2,1)S(1)} %all_to_all.39.own), channel_id=1, source_target_pairs={{0,1},{1,0},{2,3},{3,2},{4,5},{5,4},{6,7},{7,6},{8,9},{9,8},{10,11... | collective-permute-start | bytes 1572872 | tf_op jit(solution)/shard_map/ppermute | solution.py:272
  136.4 0.4 shard_map.115.first
  136.8 1.1 collective-permute-done.2.other
  137.9 1.0 shard_map.116
  (18 shorter events, 0.1 us)
Async XLA Ops:
  0.9 21.0 %copy-start.3 = (bf16[128,2048]{1,0:T(8,128)(2,1)S(1)}, bf16[128,2048]{1,0:T(8,128)(2,1)}, u32[]{:S(2)}) copy-start(bf16[128,2048]{1,0:T(8,128)(2,1)} %wk.1) | copy-start | bytes 1572868
  12.7 9.3 %copy-start.2 = (bf16[128,2048]{1,0:T(8,128)(2,1)S(1)}, bf16[128,2048]{1,0:T(8,128)(2,1)}, u32[]{:S(2)}) copy-start(bf16[128,2048]{1,0:T(8,128)(2,1)} %wq.1) | copy-start | bytes 1572868
  12.7 9.3 %collective-permute-start = (bf16[4,256,256]{2,1,0:T(8,128)(2,1)S(1)}, bf16[4,256,256]{2,1,0:T(8,128)(2,1)S(1)}, u32[]{:S(2)}, u32[]{:S(2)}) collective-permute-start(bf16[4,256,256]{2,1,0:T(8,128)(2,1)S(1)} %all_to_all.35.own), channel_id=1, source_target_pairs={{0,1},{1,0},{2,3},{3,2},{4,5},{5,4},{6,7},{7,6},{8,9},{9,8},{10,11... | collective-permute-start | bytes 1572872 | tf_op jit(solution)/shard_map/ppermute | solution.py:272
  20.4 1.5 %copy-start.5 = (f32[256,2]{0,1:T(2,128)S(1)}, f32[256,2]{0,1:T(2,128)}, u32[]{:S(2)}) copy-start(f32[256,2]{0,1:T(2,128)} %param.19) | copy-start | bytes 6148
  20.6 1.4 %copy-start.4 = (f32[2048]{0:T(1024)S(1)}, f32[2048]{0:T(1024)}, u32[]{:S(2)}) copy-start(f32[2048]{0:T(1024)} %param.12) | copy-start | bytes 24580
  22.0 0.7 copy-start.6
  22.0 0.7 copy-start.7
  61.2 24.4 %all-to-all-start.3 = ((bf16[8,16,32,128]{3,2,1,0:T(8,128)(2,1)}), bf16[8,16,32,128]{3,2,1,0:T(8,128)(2,1)S(1)}, u32[]{:S(2)}, u32[]{:S(2)}) async-start(bf16[8,16,32,128]{3,2,1,0:T(8,128)(2,1)} %broadcast_in_dim.7), calls=%async_computation.3 | async-start | bytes 2097152 | tf_op jit(solution)/shard_map/all_to_all | solution.py:268
  103.2 16.6 %all-to-all-start.5 = ((bf16[16,16,128]{2,1,0:T(8,128)(2,1)}), bf16[16,16,128]{2,1,0:T(8,128)(2,1)S(1)}, u32[]{:S(2)}, u32[]{:S(2)}) async-start(bf16[16,16,128]{2,1,0:T(8,128)(2,1)} %shard_map.113), calls=%async_computation.5 | async-start | bytes 131072 | tf_op jit(solution)/shard_map/all_to_all | solution.py:341
  108.2 2.9 %collective-permute-start.1 = (bf16[16,128]{1,0:T(8,128)(2,1)S(1)}, bf16[16,128]{1,0:T(8,128)(2,1)S(1)}, u32[]{:S(2)}, u32[]{:S(2)}) collective-permute-start(bf16[16,128]{1,0:T(8,128)(2,1)S(1)} %slice.15), channel_id=1, source_target_pairs={{0,8},{8,16},{16,24},{24,32},{32,40},{40,48},{48,56},{56,64},{64,7... | collective-permute-start | bytes 12296 | tf_op jit(solution)/shard_map/ppermute | solution.py:337
  119.9 16.5 %copy-start = (bf16[1024,256]{1,0:T(8,128)(2,1)S(1)}, bf16[1024,256]{1,0:T(8,128)(2,1)}, u32[]{:S(2)}) copy-start(bf16[1024,256]{1,0:T(8,128)(2,1)} %wpo.3) | copy-start | bytes 1572868
  119.9 16.5 %copy-start.1 = (bf16[1024,256]{1,0:T(8,128)(2,1)S(1)}, bf16[1024,256]{1,0:T(8,128)(2,1)}, u32[]{:S(2)}) copy-start(bf16[1024,256]{1,0:T(8,128)(2,1)} %wao.3) | copy-start | bytes 1572868
  129.4 8.5 %collective-permute-start.2 = (bf16[4,512,128]{2,1,0:T(8,128)(2,1)S(1)}, bf16[4,512,128]{2,1,0:T(8,128)(2,1)S(1)}, u32[]{:S(2)}, u32[]{:S(2)}) collective-permute-start(bf16[4,512,128]{2,1,0:T(8,128)(2,1)S(1)} %all_to_all.39.own), channel_id=1, source_target_pairs={{0,1},{1,0},{2,3},{3,2},{4,5},{5,4},{6,7},{7,6},{8,9},{9,8},{10,11... | collective-permute-start | bytes 1572872 | tf_op jit(solution)/shard_map/ppermute | solution.py:272
